TPU v7x, 32 devices: a whole 2x2x4 slice. The times are simulated.
32 devices in a mesh: kv: 8 (over z, y), tp: 4 (over x, core).
Axes of the slice: x: 2, y: 2, z: 4, core: 2. Of those that a mesh axis runs over, the one named last changes fastest.
Arguments:
- queries: bfloat16 [2048, 3072], P('kv', 'tp'), may hold values from -6 to 6
- key_vectors: bfloat16 [2048, 512], P('kv', 'tp'), may hold values from -6 to 6
- value_vectors: bfloat16 [2048, 512], P('kv', 'tp'), may hold values from -6 to 6
- log_sums: float32 [2048, 48], P('kv', 'tp'), may hold values from 4.5 to 6.5
- out_grad: bfloat16 [2048, 3072], P('kv', 'tp'), may hold values from -48 to 48
- layer_input: bfloat16 [2048, 3072], P('kv', 'tp'), may hold values from -0.29882812 to 0.29882812
- chosen: int32 [32, 16], P('kv'), may hold values from -1 to 55, as said below
Outputs:
- query_grad: bfloat16 [2048, 3072], P('kv', 'tp')
- key_grad: bfloat16 [2048, 512], P('kv', 'tp')
- value_grad: bfloat16 [2048, 512], P('kv', 'tp')
- weight_grad: float32 [3072, 512], P('kv', 'tp')
Inputs may be any that keep to these rules, and one draw needn't show every extreme that they name: `chosen`: each entry is -1 or the number c of a block of 32 positions (c * 32 to c * 32 + 31) that lies wholly within an earlier index of kv than its query block. The numbers of one row differ, and all query blocks held by one index of kv together take at most one block from each other index.
All inputs are finite; a program needn't handle non-finite values.
Results may differ from a plain program's by a relative error of at most 0.0061.
Values may be sent and summed in bfloat16 or wider, within the bound.
No kernel may reach another device: no remote copies, remote signals or barrier semaphores. Data moves between devices by JAX's collectives and lax.ppermute only.
A program may use at most 64 MiB of HBM per device.

v0:
```python
import jax
import jax.numpy as jnp
from jax import lax
from jax.sharding import PartitionSpec as P

HEAD = 64
KB = 32
QB = 64
NSEL = 16


def per_device(queries, key_vectors, value_vectors, log_sums, out_grad, layer_input, chosen):
    axis_count = lax.axis_size("kv")
    own_index = lax.axis_index("kv")
    span_rows = queries.shape[0]
    kv_local = key_vectors.shape[1] // HEAD
    group_size = queries.shape[1] // key_vectors.shape[1]
    blocks_here = span_rows // KB
    query_blocks = span_rows // QB
    score_scale = HEAD ** (-0.5)
    half_width = kv_local * HEAD
    pair_width = 2 * half_width
    paired = jnp.concatenate([key_vectors, value_vectors], axis=1)
    owners = jnp.arange(axis_count, dtype=jnp.int32)
    usable = chosen >= 0
    owner_of = jnp.where(usable, chosen // blocks_here, -1)
    within = chosen - chosen // blocks_here * blocks_here
    matched = owner_of[:, :, None] == owners[None, None, :]
    wanted = jnp.max(jnp.where(matched, within[:, :, None], -1), axis=(0, 1))
    incoming = lax.all_to_all(wanted[:, None], "kv", split_axis=0, concat_axis=0, tiled=True)[:, 0]
    blocks = paired.reshape(blocks_here, KB, pair_width)
    outgoing = jnp.where(
        (incoming >= 0)[:, None, None],
        blocks[jnp.maximum(incoming, 0)],
        jnp.zeros((), paired.dtype),
    )
    fetched = lax.all_to_all(outgoing, "kv", split_axis=0, concat_axis=0, tiled=True)
    query_parts = queries.reshape(query_blocks, QB, kv_local, group_size, HEAD)
    grad_parts = out_grad.reshape(query_blocks, QB, kv_local, group_size, HEAD)
    sum_parts = log_sums.reshape(query_blocks, QB, kv_local, group_size)
    slot_owner = jnp.clip(owner_of, 0, axis_count - 1)
    key_own = key_vectors.reshape(span_rows, kv_local, HEAD)
    value_own = value_vectors.reshape(span_rows, kv_local, HEAD)
    key_pos = own_index * span_rows + jnp.arange(span_rows, dtype=jnp.int32)

    def one_block(packed):
        query_part, grad_part, sum_part, slot_part, usable_part, block_index = packed
        selected = fetched[slot_part].reshape(NSEL * KB, 2, kv_local, HEAD)
        key_sel = selected[:, 0]
        value_sel = selected[:, 1]
        keep_key = jnp.repeat(usable_part, KB)
        query_pos = own_index * span_rows + block_index * QB + jnp.arange(QB, dtype=jnp.int32)
        causal = key_pos[None, :] <= query_pos[:, None]
        score_sel = (
            jnp.einsum("qhgd,khd->qhgk", query_part, key_sel, preferred_element_type=jnp.float32)
            * score_scale
        )
        score_own = (
            jnp.einsum("qhgd,khd->qhgk", query_part, key_own, preferred_element_type=jnp.float32)
            * score_scale
        )
        weight_sel = jnp.where(
            keep_key[None, None, None, :], jnp.exp(score_sel - sum_part[..., None]), 0.0
        )
        weight_own = jnp.where(
            causal[:, None, None, :], jnp.exp(score_own - sum_part[..., None]), 0.0
        )
        round_sel = weight_sel.astype(jnp.bfloat16)
        round_own = weight_own.astype(jnp.bfloat16)
        output = jnp.einsum(
            "qhgk,khd->qhgd", round_sel, value_sel, preferred_element_type=jnp.float32
        )
        output = output + jnp.einsum(
            "qhgk,khd->qhgd", round_own, value_own, preferred_element_type=jnp.float32
        )
        row_delta = jnp.sum(grad_part.astype(jnp.float32) * output, axis=-1)
        prod_sel = jnp.einsum(
            "qhgd,khd->qhgk", grad_part, value_sel, preferred_element_type=jnp.float32
        )
        prod_own = jnp.einsum(
            "qhgd,khd->qhgk", grad_part, value_own, preferred_element_type=jnp.float32
        )
        slope_sel = (weight_sel * (prod_sel - row_delta[..., None])).astype(jnp.bfloat16)
        slope_own = (weight_own * (prod_own - row_delta[..., None])).astype(jnp.bfloat16)
        query_total = jnp.einsum(
            "qhgk,khd->qhgd", slope_sel, key_sel, preferred_element_type=jnp.float32
        )
        query_total = query_total + jnp.einsum(
            "qhgk,khd->qhgd", slope_own, key_own, preferred_element_type=jnp.float32
        )
        query_out = (query_total * score_scale).astype(jnp.bfloat16)
        key_sel_grad = (
            jnp.einsum("qhgk,qhgd->khd", slope_sel, query_part, preferred_element_type=jnp.float32)
            * score_scale
        )
        value_sel_grad = jnp.einsum(
            "qhgk,qhgd->khd", round_sel, grad_part, preferred_element_type=jnp.float32
        )
        key_own_grad = (
            jnp.einsum("qhgk,qhgd->khd", slope_own, query_part, preferred_element_type=jnp.float32)
            * score_scale
        )
        value_own_grad = jnp.einsum(
            "qhgk,qhgd->khd", round_own, grad_part, preferred_element_type=jnp.float32
        )
        sel_pair = jnp.concatenate(
            [
                key_sel_grad.reshape(NSEL, KB, half_width),
                value_sel_grad.reshape(NSEL, KB, half_width),
            ],
            axis=2,
        )
        own_pair = jnp.concatenate(
            [
                key_own_grad.reshape(span_rows, half_width),
                value_own_grad.reshape(span_rows, half_width),
            ],
            axis=1,
        )
        return (query_out, sel_pair, own_pair)

    block_ids = jnp.arange(query_blocks, dtype=jnp.int32)
    query_outs, sel_pairs, own_pairs = lax.map(
        one_block, (query_parts, grad_parts, sum_parts, slot_owner, usable, block_ids)
    )
    onehot = ((slot_owner[:, :, None] == owners[None, None, :]) & usable[:, :, None]).astype(
        jnp.float32
    )
    onehot = onehot.reshape(query_blocks * NSEL, axis_count)
    per_owner = jnp.einsum(
        "so,sr->or",
        onehot,
        sel_pairs.reshape(query_blocks * NSEL, KB * pair_width),
        precision=lax.Precision.HIGHEST,
    )
    returned = lax.all_to_all(
        per_owner.reshape(axis_count, KB, pair_width), "kv", split_axis=0, concat_axis=0, tiled=True
    )
    placing = (incoming[None, :] == jnp.arange(blocks_here, dtype=jnp.int32)[:, None]).astype(
        jnp.float32
    )
    landed = jnp.einsum(
        "bs,sr->br",
        placing,
        returned.reshape(axis_count, KB * pair_width),
        precision=lax.Precision.HIGHEST,
    )
    totals = jnp.sum(own_pairs, axis=0) + landed.reshape(span_rows, pair_width)
    key_grad = totals[:, :half_width].astype(jnp.bfloat16)
    value_grad = totals[:, half_width:].astype(jnp.bfloat16)
    full_input = lax.all_gather(layer_input, "tp", axis=1, tiled=True)
    weight_grad = lax.psum_scatter(
        lax.dot_general(
            full_input, key_grad, (((0,), (0,)), ((), ())), preferred_element_type=jnp.float32
        ),
        "kv",
        scatter_dimension=0,
        tiled=True,
    )
    return (query_outs.reshape(span_rows, queries.shape[1]), key_grad, value_grad, weight_grad)


def solution(mesh):
    placed = (
        P("kv", "tp"),
        P("kv", "tp"),
        P("kv", "tp"),
        P("kv", "tp"),
        P("kv", "tp"),
        P("kv", "tp"),
        P("kv", None),
    )
    return jax.shard_map(
        per_device,
        mesh=mesh,
        in_specs=placed,
        out_specs=(P("kv", "tp"), P("kv", "tp"), P("kv", "tp"), P("kv", "tp")),
        check_vma=False,
    )
```

profile of v0, /device:TPU:0, one launch (start us, length us, event | category | flops | bytes accessed | tf_op | source)
XLA Modules:
  0.0 224.7 jit_solution(12152546866315410712)
XLA Ops:
  7.2 1.3 broadcast_clamp_fusion
  9.3 7.3 %all-to-all-start = ((s32[8,1,1]{2,1,0:T(1,128)}), s32[8,1,1]{2,1,0:T(1,128)S(1)}, u32[]{:S(2)}, u32[]{:S(2)}) async-start(s32[8,1,1]{2,1,0:T(1,128)} %copy.110), calls=%async_computation | async-start | bytes 8192 | tf_op jit(solution)/shard_map/all_to_all | solution.py:30
  17.5 5.5 %all-to-all-done = s32[8,1,1]{2,1,0:T(1,128)S(1)} async-done(((s32[8,1,1]{2,1,0:T(1,128)}), s32[8,1,1]{2,1,0:T(1,128)S(1)}, u32[]{:S(2)}, u32[]{:S(2)}) %all-to-all-start) | async-done | bytes 64 | tf_op jit(solution)/shard_map/all_to_all | solution.py:30
  24.9 3.4 %all-to-all-start.1 = ((bf16[8,32,256]{2,1,0:T(8,128)(2,1)}), bf16[8,32,256]{2,1,0:T(8,128)(2,1)S(1)}, u32[]{:S(2)}, u32[]{:S(2)}) async-start(bf16[8,32,256]{2,1,0:T(8,128)(2,1)} %broadcast_select_fusion), calls=%async_computation.1 | async-start | bytes 262144 | tf_op jit(solution)/shard_map/all_to_all | solution.py:37
  29.1 1.6 copy.113
  35.0 1.2 and.19
  36.9 93.2 %while.18 = (s32[]{:T(128)}, bf16[4,64,2,6,64]{1,4,3,2,0:T(8,128)(2,1)}, f32[4,16,32,256]{3,2,1,0:T(8,128)}, f32[4,256,256]{1,2,0:T(8,128)}, s32[4,16]{1,0:T(4,1...) while((s32[]{:T(128)}, ...), condition=%wide.region_3.4_spmd.clone.clone, body=%wide.region_1.3_spmd.clone.clone.sunk | while | flops 458359424 | bytes 25241412 | solution.py:123
  39.2 1.4 fusion.153
  42.5 1.2 fusion.154
  43.8 1.3 fusion.155
  45.1 1.3 fusion.156
  46.3 1.2 fusion.159
  48.6 2.0 reshape.226
  50.6 1.2 convolution_bitcast_fusion.14
  53.7 1.2 fusion.157
  58.5 1.8 fusion.158
  62.5 1.4 fusion.153
  65.8 1.2 fusion.154
  67.0 1.3 fusion.155
  68.3 1.3 fusion.156
  69.6 1.2 fusion.159
  71.9 2.0 reshape.226
  73.9 1.2 convolution_bitcast_fusion.14
  76.9 1.2 fusion.157
  81.7 1.8 fusion.158
  85.8 1.4 fusion.153
  89.0 1.2 fusion.154
  90.3 1.3 fusion.155
  91.6 1.3 fusion.156
  92.9 1.2 fusion.159
  95.1 2.0 reshape.226
  97.2 1.2 convolution_bitcast_fusion.14
  100.2 1.2 fusion.157
  105.0 1.8 fusion.158
  109.1 1.4 fusion.153
  113.6 1.3 fusion.155
  114.9 1.3 fusion.156
  116.2 1.2 fusion.159
  118.4 2.0 reshape.226
  123.5 1.2 fusion.157
  128.3 1.8 fusion.158
  130.1 3.5 %fusion.66 = f32[8,32,256]{2,0,1:T(8,128)S(1)} fusion(s32[64]{0:T(128)} %eq.51, pred[64]{0:T(512)(128)(4,1)} %and.19, f32[8,8,32,256]{3,2,1,0:T(8,128)} %bitcast.274), kind=kOutput, calls=%fused_computation.90 | convolution fusion | flops 50332672 | bytes 2359616 | tf_op jit(solution)/shard_map/so,sr->or/dot_general | solution.py:130
  134.5 5.9 %all-to-all-start.2 = ((f32[8,32,256]{2,1,0:T(8,128)}), f32[8,32,256]{2,1,0:T(8,128)S(1)}, u32[]{:S(2)}, u32[]{:S(2)}) async-start(f32[8,32,256]{2,1,0:T(8,128)} %copy.120), calls=%async_computation.2 | async-start | bytes 524288 | tf_op jit(solution)/shard_map/all_to_all | solution.py:136
  140.7 7.9 %all-to-all-done.2 = f32[8,32,256]{2,1,0:T(8,128)S(1)} async-done(((f32[8,32,256]{2,1,0:T(8,128)}), f32[8,32,256]{2,1,0:T(8,128)S(1)}, u32[]{:S(2)}, u32[]{:S(2)}) %all-to-all-start.2) | async-done | bytes 262176 | tf_op jit(solution)/shard_map/all_to_all | solution.py:136
  149.3 2.9 %convolution_bitcast_fusion.8 = f32[3072,128]{0,1:T(8,128)} fusion(bf16[256,3072]{1,0:T(8,128)(2,1)} %all-gather.2.cloned.1.call-done, bf16[256,256]{0,1:T(8,128)(2,1)S(1)} %add_convert_fusion), kind=kOutput, calls=%fused_computation.89 | convolution fusion | flops 201326592 | bytes 3211264 | tf_op jit(solution)/shard_map/dot_general | solution.py:153
  154.3 1.4 reshape.213
  157.2 58.9 %reduce-scatter.2.cloned.1.call-done = f32[384,128]{0,1:T(8,128)} async-done(((f32[3072,128]{0,1:T(8,128)}), f32[384,128]{0,1:T(8,128)}) %reduce-scatter.2.cloned.1.call-update) | async-done | bytes 196624 | tf_op jit(solution)/shard_map/reduce_scatter | solution.py:152
  216.1 1.7 copy.125
  (206 shorter events, 55.8 us)
Async XLA Ops:
  7.2 23.5 %copy-start.7 = (bf16[256,128]{1,0:T(8,128)(2,1)S(1)}, bf16[256,128]{1,0:T(8,128)(2,1)}, u32[]{:S(2)}) copy-start(bf16[256,128]{1,0:T(8,128)(2,1)} %param.11) | copy-start | bytes 196612
  7.2 24.2 %copy-start.5 = (bf16[256,768]{1,0:T(8,128)(2,1)S(1)}, bf16[256,768]{1,0:T(8,128)(2,1)}, u32[]{:S(2)}) copy-start(bf16[256,768]{1,0:T(8,128)(2,1)} %param.9) | copy-start | bytes 1179652
  9.3 13.7 %all-to-all-start = ((s32[8,1,1]{2,1,0:T(1,128)}), s32[8,1,1]{2,1,0:T(1,128)S(1)}, u32[]{:S(2)}, u32[]{:S(2)}) async-start(s32[8,1,1]{2,1,0:T(1,128)} %copy.110), calls=%async_computation | async-start | bytes 8192 | tf_op jit(solution)/shard_map/all_to_all | solution.py:30
  24.9 12.0 %all-to-all-start.1 = ((bf16[8,32,256]{2,1,0:T(8,128)(2,1)}), bf16[8,32,256]{2,1,0:T(8,128)(2,1)S(1)}, u32[]{:S(2)}, u32[]{:S(2)}) async-start(bf16[8,32,256]{2,1,0:T(8,128)(2,1)} %broadcast_select_fusion), calls=%async_computation.1 | async-start | bytes 262144 | tf_op jit(solution)/shard_map/all_to_all | solution.py:37
  28.3 120.9 %all-gather.2.cloned.1.call-start = ((), (), s32[]{:S(2)}) async-start(), calls=%async_computation.4 | async-start | bytes 1966080 | tf_op jit(solution)/shard_map/all_gather | solution.py:151
  31.4 1.8 copy-start.6
  33.2 1.8 copy-start.10
  36.9 2.3 %copy-start.8 = (f32[4,64,2,6]{1,0,3,2:T(4,128)}, f32[4,64,2,6]{1,0,3,2:T(4,128)S(1)}, u32[]{:S(2)}) copy-start(f32[4,64,2,6]{1,0,3,2:T(4,128)S(1)} %get-tuple-element.488) | copy-start | bytes 36868 | tf_op jit(solution)/shard_map/while
  36.9 4.2 %copy-start.11 = (s32[4]{0:T(128)}, s32[4]{0:T(128)S(1)}, u32[]{:S(2)}) copy-start(s32[4]{0:T(128)S(1)} %get-tuple-element.490) | copy-start | bytes 52 | tf_op jit(solution)/shard_map/while
  38.3 2.3 %copy-start.1 = (bf16[512,1,2,64]{0,3,2,1:T(8,128)(2,1)}, bf16[512,1,2,64]{0,3,2,1:T(8,128)(2,1)S(1)}, u32[]{:S(2)}) copy-start(bf16[512,1,2,64]{0,3,2,1:T(8,128)(2,1)S(1)} %copy.168) | copy-start | bytes 393220 | tf_op jit(solution)/shard_map/while
  51.9 1.0 copy-start
  53.6 4.3 %copy-start.2 = (bf16[512,1,2,64]{0,3,2,1:T(8,128)(2,1)S(1)}, bf16[512,1,2,64]{0,3,2,1:T(8,128)(2,1)}, u32[]{:S(2)}) copy-start(bf16[512,1,2,64]{0,3,2,1:T(8,128)(2,1)} %copy-done.1) | copy-start | bytes 393220 | tf_op jit(solution)/shard_map/while
  57.2 3.1 %copy-start.9 = (f32[4,64,2,6]{1,0,3,2:T(4,128)S(1)}, f32[4,64,2,6]{1,0,3,2:T(4,128)}, u32[]{:S(2)}) copy-start(f32[4,64,2,6]{1,0,3,2:T(4,128)} %copy-done.8) | copy-start | bytes 36868 | tf_op jit(solution)/shard_map/while
  57.2 3.1 %copy-start.12 = (s32[4]{0:T(128)S(1)}, s32[4]{0:T(128)}, u32[]{:S(2)}) copy-start(s32[4]{0:T(128)} %copy-done.11) | copy-start | bytes 52 | tf_op jit(solution)/shard_map/while
  60.3 2.3 %copy-start.8 = (f32[4,64,2,6]{1,0,3,2:T(4,128)}, f32[4,64,2,6]{1,0,3,2:T(4,128)S(1)}, u32[]{:S(2)}) copy-start(f32[4,64,2,6]{1,0,3,2:T(4,128)S(1)} %get-tuple-element.488) | copy-start | bytes 36868 | tf_op jit(solution)/shard_map/while
  60.3 4.1 %copy-start.11 = (s32[4]{0:T(128)}, s32[4]{0:T(128)S(1)}, u32[]{:S(2)}) copy-start(s32[4]{0:T(128)S(1)} %get-tuple-element.490) | copy-start | bytes 52 | tf_op jit(solution)/shard_map/while
  61.7 2.2 copy-start.1
  75.1 1.0 copy-start
  76.9 4.3 %copy-start.2 = (bf16[512,1,2,64]{0,3,2,1:T(8,128)(2,1)S(1)}, bf16[512,1,2,64]{0,3,2,1:T(8,128)(2,1)}, u32[]{:S(2)}) copy-start(bf16[512,1,2,64]{0,3,2,1:T(8,128)(2,1)} %copy-done.1) | copy-start | bytes 393220 | tf_op jit(solution)/shard_map/while
  80.5 3.1 %copy-start.9 = (f32[4,64,2,6]{1,0,3,2:T(4,128)S(1)}, f32[4,64,2,6]{1,0,3,2:T(4,128)}, u32[]{:S(2)}) copy-start(f32[4,64,2,6]{1,0,3,2:T(4,128)} %copy-done.8) | copy-start | bytes 36868 | tf_op jit(solution)/shard_map/while
  80.5 3.1 %copy-start.12 = (s32[4]{0:T(128)S(1)}, s32[4]{0:T(128)}, u32[]{:S(2)}) copy-start(s32[4]{0:T(128)} %copy-done.11) | copy-start | bytes 52 | tf_op jit(solution)/shard_map/while
  83.5 2.3 %copy-start.8 = (f32[4,64,2,6]{1,0,3,2:T(4,128)}, f32[4,64,2,6]{1,0,3,2:T(4,128)S(1)}, u32[]{:S(2)}) copy-start(f32[4,64,2,6]{1,0,3,2:T(4,128)S(1)} %get-tuple-element.488) | copy-start | bytes 36868 | tf_op jit(solution)/shard_map/while
  83.5 4.1 %copy-start.11 = (s32[4]{0:T(128)}, s32[4]{0:T(128)S(1)}, u32[]{:S(2)}) copy-start(s32[4]{0:T(128)S(1)} %get-tuple-element.490) | copy-start | bytes 52 | tf_op jit(solution)/shard_map/while
  84.9 2.2 copy-start.1
  98.4 1.0 copy-start
  100.2 4.3 %copy-start.2 = (bf16[512,1,2,64]{0,3,2,1:T(8,128)(2,1)S(1)}, bf16[512,1,2,64]{0,3,2,1:T(8,128)(2,1)}, u32[]{:S(2)}) copy-start(bf16[512,1,2,64]{0,3,2,1:T(8,128)(2,1)} %copy-done.1) | copy-start | bytes 393220 | tf_op jit(solution)/shard_map/while
  103.8 3.1 %copy-start.9 = (f32[4,64,2,6]{1,0,3,2:T(4,128)S(1)}, f32[4,64,2,6]{1,0,3,2:T(4,128)}, u32[]{:S(2)}) copy-start(f32[4,64,2,6]{1,0,3,2:T(4,128)} %copy-done.8) | copy-start | bytes 36868 | tf_op jit(solution)/shard_map/while
  103.8 3.1 %copy-start.12 = (s32[4]{0:T(128)S(1)}, s32[4]{0:T(128)}, u32[]{:S(2)}) copy-start(s32[4]{0:T(128)} %copy-done.11) | copy-start | bytes 52 | tf_op jit(solution)/shard_map/while
  106.9 2.3 %copy-start.8 = (f32[4,64,2,6]{1,0,3,2:T(4,128)}, f32[4,64,2,6]{1,0,3,2:T(4,128)S(1)}, u32[]{:S(2)}) copy-start(f32[4,64,2,6]{1,0,3,2:T(4,128)S(1)} %get-tuple-element.488) | copy-start | bytes 36868 | tf_op jit(solution)/shard_map/while
  106.9 4.1 %copy-start.11 = (s32[4]{0:T(128)}, s32[4]{0:T(128)S(1)}, u32[]{:S(2)}) copy-start(s32[4]{0:T(128)S(1)} %get-tuple-element.490) | copy-start | bytes 52 | tf_op jit(solution)/shard_map/while
  108.2 2.2 copy-start.1
  121.7 1.0 copy-start
  123.5 4.3 %copy-start.2 = (bf16[512,1,2,64]{0,3,2,1:T(8,128)(2,1)S(1)}, bf16[512,1,2,64]{0,3,2,1:T(8,128)(2,1)}, u32[]{:S(2)}) copy-start(bf16[512,1,2,64]{0,3,2,1:T(8,128)(2,1)} %copy-done.1) | copy-start | bytes 393220 | tf_op jit(solution)/shard_map/while
  127.0 3.1 %copy-start.9 = (f32[4,64,2,6]{1,0,3,2:T(4,128)S(1)}, f32[4,64,2,6]{1,0,3,2:T(4,128)}, u32[]{:S(2)}) copy-start(f32[4,64,2,6]{1,0,3,2:T(4,128)} %copy-done.8) | copy-start | bytes 36868 | tf_op jit(solution)/shard_map/while
  127.0 3.1 %copy-start.12 = (s32[4]{0:T(128)S(1)}, s32[4]{0:T(128)}, u32[]{:S(2)}) copy-start(s32[4]{0:T(128)} %copy-done.11) | copy-start | bytes 52 | tf_op jit(solution)/shard_map/while
  130.1 10.5 %copy-start.3 = (f32[4,256,256]{1,2,0:T(8,128)S(1)}, f32[4,256,256]{1,2,0:T(8,128)}, u32[]{:S(2)}) copy-start(f32[4,256,256]{1,2,0:T(8,128)} %get-tuple-element.178) | copy-start | bytes 3145732
  134.5 14.1 %all-to-all-start.2 = ((f32[8,32,256]{2,1,0:T(8,128)}), f32[8,32,256]{2,1,0:T(8,128)S(1)}, u32[]{:S(2)}, u32[]{:S(2)}) async-start(f32[8,32,256]{2,1,0:T(8,128)} %copy.120), calls=%async_computation.2 | async-start | bytes 524288 | tf_op jit(solution)/shard_map/all_to_all | solution.py:136
  140.4 75.8 %reduce-scatter.2.cloned.1.call-start = ((), (), s32[]{:S(2)}) async-start(), calls=%async_computation.5 | async-start | bytes 1769472 | tf_op jit(solution)/shard_map/reduce_scatter | solution.py:152
  152.2 1.1 copy-start.4
Sparse Core Ops, SparseCore 0:
  30.7 20.9 all-gather.1
  152.3 63.7 reduce-scatter.1
where the time goes:
time: 227 us; the launch traced here: 225 us
  waiting for transfers between devices  73.1 us (32%)
  matrix products  62.1 us (27%)
  local copies, waits for them, and re-layouts  44.4 us (20%)
  starting transfers between devices  16.9 us (7%)
  between operations  14.2 us (6%)
  other arithmetic  10.4 us (5%)
  loops' own time  3.57 us (2%)
    reduce_scatter x1, waiting for transfers between devices, per_device(): lax.psum_scatter(lax.dot_general(full_input, key_grad, (((0,), (0,)), (()...  58.9 us
    unnamed x22, local copies, waits for them, and re-layouts  11.4 us
    reshape x4, local copies, waits for them, and re-layouts, one_block(): key_sel_grad.reshape(NSEL, KB, half_width)  8.17 us
    all_to_all x1, waiting for transfers between devices, per_device(): lax.all_to_all(per_owner.reshape(axis_count, KB, pair_width), 'kv', split...  7.9 us
    dot_general x4, matrix products, one_block(): jnp.einsum('qhgk,khd->qhgd', slope_own, key_own, preferred_element_type=j...  7.34 us
    all_to_all x1, starting transfers between devices, per_device(): lax.all_to_all(wanted[:, None], 'kv', split_axis=0, concat_axis=0, tiled=...  7.31 us
    dynamic_update_slice x8, other arithmetic, per_device(): lax.map(one_block, (query_parts, grad_parts, sum_parts, slot_owner, usabl...  6.22 us
    all_to_all x1, starting transfers between devices, per_device(): lax.all_to_all(per_owner.reshape(axis_count, KB, pair_width), 'kv', split...  5.91 us
  transfers between devices with their start and end apart: 5, of which 3 were waited for; matrix products, arithmetic and copies ran while one was open for 47% of the time, Pallas kernels for 0%

commit v1 on v0

v1 whole, which is shorter than its diff:
```python
import math

import jax
import jax.numpy as jnp
from jax import lax
from jax.experimental import pallas as pl
from jax.experimental.pallas import tpu as pltpu
from jax.sharding import PartitionSpec as P

HEAD = 64
KB = 32
QB = 64
PAD_ROWS = 16
MASKED = -1e30


def dot_nt(a, b):
    return lax.dot_general(a, b, (((1,), (1,)), ((), ())), preferred_element_type=jnp.float32)


def dot_nn(a, b):
    return lax.dot_general(a, b, (((1,), (0,)), ((), ())), preferred_element_type=jnp.float32)


def dot_tn(a, b):
    return lax.dot_general(a, b, (((0,), (0,)), ((), ())), preferred_element_type=jnp.float32)


def attention_kernel(wanted, q_ref, g_ref, kv_ref, all_ref, sums_ref, bias_ref,
                     dq_ref, own_ref, sel_ref,
                     kv_sel, dk_own, dv_own, dk_sel, dv_sel, p_buf, dp_buf):
    span = q_ref.shape[0]
    half = kv_ref.shape[1] // 2
    kv_local = half // HEAD
    group = q_ref.shape[1] // half
    blocks = span // QB
    owners = all_ref.shape[0]
    scale = HEAD ** -0.5
    chunk = math.gcd(owners, 8) * KB
    chunks = owners * KB // chunk

    def fetch(o, carry):
        first = pl.multiple_of(jnp.maximum(wanted[o], 0) * KB, KB)
        kv_sel[pl.ds(pl.multiple_of(o * KB, KB), KB), :] = all_ref[o, pl.ds(first, KB), :]
        return carry

    if owners <= 8:
        for o in range(owners):
            fetch(o, 0)
    else:
        lax.fori_loop(0, owners, fetch, 0)

    def over_chunks(body, init):
        if chunks == 1:
            return body(0, init)
        return lax.fori_loop(0, chunks, body, init)

    key_id = lax.broadcasted_iota(jnp.int32, (QB, group * QB), 0)
    query_id = lax.broadcasted_iota(jnp.int32, (QB, group * QB), 1) % QB
    causal = key_id <= query_id

    for h in range(kv_local):
        k_lanes = slice(h * HEAD, (h + 1) * HEAD)
        v_lanes = slice(half + h * HEAD, half + (h + 1) * HEAD)
        for b in range(blocks):
            rows = slice(b * QB, (b + 1) * QB)
            heads = [h * group + i for i in range(group)]
            qs = jnp.concatenate([q_ref[rows, i * HEAD:(i + 1) * HEAD] for i in heads], axis=0)
            gs = jnp.concatenate([g_ref[rows, i * HEAD:(i + 1) * HEAD] for i in heads], axis=0)
            sums = sums_ref[h * blocks + b:h * blocks + b + 1, :]
            n_own = (b + 1) * QB
            k_own = kv_ref[:n_own, k_lanes]
            v_own = kv_ref[:n_own, v_lanes]
            p_own = jnp.exp(dot_nt(k_own, qs) * scale - sums)
            last = jnp.where(causal, p_own[b * QB:, :], 0.0)
            p_own = jnp.concatenate([p_own[:b * QB, :], last], axis=0) if b else last
            dp_own = dot_nt(v_own, gs)
            p16_own = p_own.astype(jnp.bfloat16)
            delta = jnp.sum(p16_own.astype(jnp.float32) * dp_own, axis=0, keepdims=True)

            def first_pass(c, delta):
                at = pl.ds(c * chunk, chunk)
                s = dot_nt(kv_sel[at, k_lanes], qs) * scale - sums
                p = jnp.exp(s + bias_ref[at, b:b + 1])
                dp = dot_nt(kv_sel[at, v_lanes], gs)
                p_buf[at, :] = p
                dp_buf[at, :] = dp
                p16 = p.astype(jnp.bfloat16)
                dv = dot_nn(p16, gs)
                dv_sel[h, at, :] = dv if b == 0 else dv_sel[h, at, :] + dv
                return delta + jnp.sum(p16.astype(jnp.float32) * dp, axis=0, keepdims=True)

            delta = over_chunks(first_pass, delta)
            ds_own = (p_own * (dp_own - delta)).astype(jnp.bfloat16)
            dqt = dot_tn(k_own, ds_own)
            dk = dot_nn(ds_own, qs)
            dv = dot_nn(p16_own, gs)
            if b:
                dk_own[h, :b * QB, :] += dk[:b * QB]
                dv_own[h, :b * QB, :] += dv[:b * QB]
            dk_own[h, b * QB:n_own, :] = dk[b * QB:]
            dv_own[h, b * QB:n_own, :] = dv[b * QB:]

            def second_pass(c, dqt):
                at = pl.ds(c * chunk, chunk)
                ds = (p_buf[at, :] * (dp_buf[at, :] - delta)).astype(jnp.bfloat16)
                dk = dot_nn(ds, qs)
                dk_sel[h, at, :] = dk if b == 0 else dk_sel[h, at, :] + dk
                return dqt + dot_tn(kv_sel[at, k_lanes], ds)

            dqt = over_chunks(second_pass, dqt)
            dq = (dqt * scale).T
            dq = jnp.concatenate([dq[i * QB:(i + 1) * QB] for i in range(group)], axis=1)
            dq_ref[rows, h * group * HEAD:(h + 1) * group * HEAD] = dq.astype(jnp.bfloat16)
    own_ref[...] = jnp.concatenate(
        [dk_own[h] * scale for h in range(kv_local)] + [dv_own[h] for h in range(kv_local)], axis=1)
    sel_ref[...] = jnp.concatenate(
        [dk_sel[h] * scale for h in range(kv_local)] + [dv_sel[h] for h in range(kv_local)],
        axis=1).astype(sel_ref.dtype)


def landing_kernel(incoming, own_ref, back_ref, x_ref, dk_ref, dv_ref, part_ref, total):
    half = dk_ref.shape[1]
    owners = back_ref.shape[0]
    total[...] = own_ref[...]

    def land(s, carry):
        at = pl.ds(pl.multiple_of(jnp.maximum(incoming[s], 0) * KB, KB), KB)
        total[at, :] += back_ref[s].astype(jnp.float32)
        return carry

    if owners <= 8:
        for s in range(owners):
            land(s, 0)
    else:
        lax.fori_loop(0, owners, land, 0)
    dk = total[:, :half].astype(jnp.bfloat16)
    dk_ref[...] = dk
    dv_ref[...] = total[:, half:].astype(jnp.bfloat16)
    width = part_ref.shape[2]
    part = dot_tn(dk, x_ref[...]).astype(part_ref.dtype)
    for i in range(owners):
        part_ref[i] = part[:, i * width:(i + 1) * width]


def sum_kernel(parts_ref, out_ref):
    acc = parts_ref[0].astype(jnp.float32)
    for i in range(1, parts_ref.shape[0]):
        acc = acc + parts_ref[i].astype(jnp.float32)
    out_ref[...] = acc.T


def per_device(queries, key_vectors, value_vectors, log_sums, out_grad, layer_input, chosen):
    owners = lax.axis_size("kv")
    me = lax.axis_index("kv")
    span, width = queries.shape
    half = key_vectors.shape[1]
    kv_local = half // HEAD
    group = width // half
    blocks = span // QB
    blocks_here = span // KB
    f32, bf16 = jnp.float32, jnp.bfloat16
    vmem = pl.BlockSpec(memory_space=pltpu.VMEM)
    smem = pl.BlockSpec(memory_space=pltpu.SMEM)

    ids = jnp.arange(owners, dtype=jnp.int32)
    owner_of = jnp.where(chosen >= 0, chosen // blocks_here, -1)
    matched = owner_of[:, :, None] == ids[None, None, :]
    within = (chosen % blocks_here)[:, :, None]
    wanted = jnp.max(jnp.where(matched, within, -1), axis=(0, 1))
    used = jnp.any(matched, axis=1)
    bias = jnp.repeat(jnp.where(used, 0.0, MASKED).T, KB, axis=0)

    paired = jnp.concatenate([key_vectors, value_vectors], axis=1)
    note_rows = -(-owners // (2 * half * PAD_ROWS)) * PAD_ROWS
    note = jnp.pad(wanted.astype(bf16), (0, note_rows * 2 * half - owners)).reshape(note_rows, 2 * half)
    sent = jnp.concatenate([paired, note], axis=0)
    everyone = lax.all_gather(sent, "kv", axis=0, tiled=False)
    incoming = lax.dynamic_index_in_dim(
        everyone[:, span:, :].reshape(owners, -1), me, axis=1, keepdims=False).astype(jnp.int32)
    full_input = lax.all_gather(layer_input, "tp", axis=1, tiled=True)
    sums = log_sums.reshape(blocks, QB, kv_local, group).transpose(2, 0, 3, 1).reshape(
        kv_local * blocks, group * QB)

    query_grad, own, sel = pl.pallas_call(
        attention_kernel,
        name="attention",
        out_shape=(
            jax.ShapeDtypeStruct((span, width), bf16),
            jax.ShapeDtypeStruct((span, 2 * half), f32),
            jax.ShapeDtypeStruct((owners * KB, 2 * half), bf16),
        ),
        in_specs=[smem] + [vmem] * 6,
        out_specs=(vmem,) * 3,
        scratch_shapes=[
            pltpu.VMEM((owners * KB, 2 * half), bf16),
            pltpu.VMEM((kv_local, span, HEAD), f32),
            pltpu.VMEM((kv_local, span, HEAD), f32),
            pltpu.VMEM((kv_local, owners * KB, HEAD), f32),
            pltpu.VMEM((kv_local, owners * KB, HEAD), f32),
            pltpu.VMEM((owners * KB, group * QB), f32),
            pltpu.VMEM((owners * KB, group * QB), f32),
        ],
    )(wanted, queries, out_grad, paired, everyone, sums, bias)

    back = lax.all_to_all(sel.reshape(owners, KB, 2 * half), "kv", split_axis=0, concat_axis=0, tiled=True)
    rows = full_input.shape[1] // owners
    key_grad, value_grad, parts = pl.pallas_call(
        landing_kernel,
        name="landing",
        out_shape=(
            jax.ShapeDtypeStruct((span, half), bf16),
            jax.ShapeDtypeStruct((span, half), bf16),
            jax.ShapeDtypeStruct((owners, half, rows), bf16),
        ),
        in_specs=[smem] + [vmem] * 3,
        out_specs=(vmem,) * 3,
        scratch_shapes=[pltpu.VMEM((span, 2 * half), f32)],
    )(incoming, own, back, full_input)
    parts = lax.all_to_all(parts, "kv", split_axis=0, concat_axis=0, tiled=True)
    weight_grad = pl.pallas_call(
        sum_kernel,
        name="sum_parts",
        out_shape=jax.ShapeDtypeStruct((rows, half), f32),
        in_specs=[vmem],
        out_specs=vmem,
    )(parts)
    return (query_grad, key_grad, value_grad, weight_grad)


def solution(mesh):
    placed = (P("kv", "tp"),) * 6 + (P("kv", None),)
    return jax.shard_map(
        per_device,
        mesh=mesh,
        in_specs=placed,
        out_specs=(P("kv", "tp"),) * 4,
        check_vma=False,
    )
```

time: 227 us -> 112 us (0.49)
  matrix products: 62.1 us -> 0 us
  local copies, waits for them, and re-layouts: 44.4 us -> 5.3 us
  blocking collectives: 0 us -> 26.1 us
  waiting for transfers between devices: 73.1 us -> 48 us
  starting transfers between devices: 16.9 us -> 3.45 us
  Pallas kernels: 0 us -> 12.5 us
  other arithmetic: 10.4 us -> 2.27 us
  loops' own time: 3.57 us -> 0 us
    dot_general x51 -> x0, matrix products: 62.1 us -> none  [the longest x4 7.34 us: one_block(): jnp.einsum('qhgk,khd->qhgd', slope_own, key_own, preferred_element_type=j...]
    reduce_scatter x1 -> x0, waiting for transfers between devices: 58.9 us -> none  [per_device(): lax.psum_scatter(lax.dot_general(full_input, key_grad, (((0,), (0,)), (()...]
    all_gather x0 -> x1, waiting for transfers between devices: none -> 41.2 us  [per_device(): everyone = lax.all_gather(sent, 'kv', axis=0, tiled=False)]
    all_to_all x0 -> x1, blocking collectives: none -> 26.1 us  [per_device(): parts = lax.all_to_all(parts, 'kv', split_axis=0, concat_axis=0, tiled=True)]
    all_to_all x3 -> x1, starting transfers between devices: 16.6 us -> 3.37 us  [per_device(): lax.all_to_all(sel.reshape(owners, KB, 2 * half), 'kv', split_axis=0, con...]
    pallas_call x0 -> x3, Pallas kernels: none -> 12.5 us  [the longest x1 7.6 us: per_device(): pl.pallas_call(attention_kernel, name='attention', out_shape=(jax.ShapeDt...]
    unnamed x22 -> x7, local copies, waits for them, and re-layouts: 11.4 us -> 0.86 us
    reshape x17 -> x5, local copies, waits for them, and re-layouts: 11.9 us -> 1.98 us  [the longest x3 1.48 us: per_device(): log_sums.reshape(blocks, QB, kv_local, group).transpose(2, 0, 3, 1)]
  transfers between devices with their start and end apart: 5 -> 3, of which waited for: 3 -> 3; matrix products, arithmetic and copies ran while one was open for 47% -> 4% of each run, Pallas kernels for 0% -> 7%
where the time goes in v1:
time: 112 us
  waiting for transfers between devices  48 us (43%)
  blocking collectives  26.1 us (23%)
  between operations  14.1 us (13%)
  Pallas kernels  12.5 us (11%)
  local copies, waits for them, and re-layouts  5.3 us (5%)
  starting transfers between devices  3.45 us (3%)
  other arithmetic  2.27 us (2%)
    all_gather x1, waiting for transfers between devices, per_device(): everyone = lax.all_gather(sent, 'kv', axis=0, tiled=False)  41.2 us
    all_to_all x1, blocking collectives, per_device(): parts = lax.all_to_all(parts, 'kv', split_axis=0, concat_axis=0, tiled=True)  26.1 us
    pallas_call x1, Pallas kernels, per_device(): pl.pallas_call(attention_kernel, name='attention', out_shape=(jax.ShapeDt...  7.6 us
    all_to_all x1, waiting for transfers between devices, per_device(): lax.all_to_all(sel.reshape(owners, KB, 2 * half), 'kv', split_axis=0, con...  5.33 us
    all_to_all x1, starting transfers between devices, per_device(): lax.all_to_all(sel.reshape(owners, KB, 2 * half), 'kv', split_axis=0, con...  3.37 us
    pallas_call x1, Pallas kernels, per_device(): pl.pallas_call(landing_kernel, name='landing', out_shape=(jax.ShapeDtypeS...  2.93 us
  transfers between devices with their start and end apart: 3, of which 3 were waited for; matrix products, arithmetic and copies ran while one was open for 4% of the time, Pallas kernels for 7%

profile of v1, /device:TPU:0, one launch (start us, length us, event | category | flops | bytes accessed | tf_op | source)
XLA Modules:
  0.0 111.8 jit_solution(11060446228521217571)
XLA Ops:
  7.2 0.0 all-gather.6.cloned.1.call-start
  7.2 0.7 fusion.1
  7.9 0.9 constant_dynamic-update-slice_fusion.1
  8.8 0.1 select_reduce_fusion.wanted
  8.9 0.0 copy-start.2
  8.9 0.9 constant_dynamic-update-slice_fusion.kv_ref
  9.8 0.0 copy-start
  9.8 0.7 pad_maximum_fusion
  10.5 0.0 all-gather.6.cloned.1.call-update
  10.5 0.0 all-gather.4.cloned.1.call-start
  10.6 0.7 all-gather.4.cloned.1.call-update
  11.3 0.8 reshape.31
  12.1 0.7 reshape.32.sums_ref
  12.7 0.2 fusion
  12.9 0.1 copy.16
  13.0 41.2 %all-gather.6.cloned.1.call-done = bf16[2176,256]{1,0:T(8,128)(2,1)} async-done(((bf16[272,256]{1,0:T(8,128)(2,1)}), bf16[2176,256]{1,0:T(8,128)(2,1)}) %all-gather.6.cloned.1.call-update) | async-done | bytes 1114128 | tf_op jit(solution)/shard_map/all_gather | solution.py:178
  54.2 0.7 broadcast_in_dim.32
  54.9 0.0 copy-done.2
  54.9 0.0 copy-done
  54.9 7.6 %attention.1 = (bf16[256,768]{1,0:T(8,128)(2,1)}, f32[256,256]{1,0:T(8,128)}, bf16[256,256]{1,0:T(8,128)(2,1)}) custom-call(s32[8]{0:T(128)} %copy-done.2, bf16[256,768]{1,0:T(8,128)(2,1)} %q_ref.1, bf16[256,768]{1,0:T(8,128)(2,1)} %g_ref.1, bf16[256,256]{1,0:T(8,128)(2,1)} %copy-done, bf16[8,272,256]{2,1,0:T(8,128)(2,1)} %bitcast.14, ...), custom_call_target="tpu_custom_call" | custom-call | tf_op jit(solution)/shard_map/attention/pallas_call | solution.py:185
  62.5 3.4 %all-to-all-start = ((bf16[8,32,256]{2,1,0:T(8,128)(2,1)}), bf16[8,32,256]{2,1,0:T(8,128)(2,1)S(1)}, u32[]{:S(2)}, u32[]{:S(2)}) async-start(bf16[8,32,256]{2,1,0:T(8,128)(2,1)} %bitcast.19), calls=%async_computation | async-start | bytes 262144 | tf_op jit(solution)/shard_map/all_to_all | solution.py:206
  65.9 0.9 slice.4
  66.7 0.5 copy.18
  67.2 0.6 bitcast_convert_fusion.incoming
  67.8 5.3 %all-to-all-done.back_ref = bf16[8,32,256]{2,1,0:T(8,128)(2,1)S(1)} async-done(((bf16[8,32,256]{2,1,0:T(8,128)(2,1)}), bf16[8,32,256]{2,1,0:T(8,128)(2,1)S(1)}, u32[]{:S(2)}, u32[]{:S(2)}) %all-to-all-start) | async-done | bytes 131104 | tf_op jit(solution)/shard_map/all_to_all | solution.py:206
  73.2 0.0 copy-start.1
  73.2 0.7 all-gather.4.cloned.1.call-done.x_ref
  73.9 0.0 copy-done.1
  73.9 2.9 %landing.1 = (bf16[256,128]{1,0:T(8,128)(2,1)}, bf16[256,128]{1,0:T(8,128)(2,1)}, bf16[8,128,384]{2,1,0:T(8,128)(2,1)}) custom-call(s32[8]{0:T(128)} %bitcast_convert_fusion.incoming, f32[256,256]{1,0:T(8,128)} %get-tuple-element.11.own_ref, bf16[8,32,256]{2,1,0:T(8,128)(2,1)} %copy-done.1, bf16[256,3072]{1,0:T(8,128)(2,1)} %all-gather.4.cloned.1.call-done.x_ref), custom_call_target="tpu_custom_call" | custom-call | tf_op jit(solution)/shard_map/landing/pallas_call | solution.py:208
  76.8 26.1 %all_to_all.10.parts_ref = bf16[8,128,384]{2,1,0:T(8,128)(2,1)} all-to-all(bf16[8,128,384]{2,1,0:T(8,128)(2,1)} %get-tuple-element.15), channel_id=1, replica_groups=mesh['kv'=8,'tp'=4] {'kv'}, dimensions={0} | all-to-all | bytes 1572864 | tf_op jit(solution)/shard_map/all_to_all | solution.py:220
  102.9 2.0 %sum_parts.1 = f32[384,128]{1,0:T(8,128)} custom-call(bf16[8,128,384]{2,1,0:T(8,128)(2,1)} %all_to_all.10.parts_ref), custom_call_target="tpu_custom_call" | custom-call | tf_op jit(solution)/shard_map/sum_parts/pallas_call | solution.py:221
  (5 shorter events, 0.0 us)
Async XLA Ops:
  7.2 47.1 %all-gather.6.cloned.1.call-start = ((), (), s32[]{:S(2)}) async-start(), calls=%async_computation.3 | async-start | bytes 1253376 | tf_op jit(solution)/shard_map/all_gather | solution.py:178
  8.9 46.0 %copy-start.2 = (s32[8]{0:T(128)}, s32[8]{0:T(128)S(1)}, u32[]{:S(2)}) copy-start(s32[8]{0:T(128)S(1)} %select_reduce_fusion.wanted) | copy-start | bytes 100
  9.8 45.1 %copy-start = (bf16[256,256]{1,0:T(8,128)(2,1)}, bf16[256,256]{1,0:T(8,128)(2,1)S(1)}, u32[]{:S(2)}) copy-start(bf16[256,256]{1,0:T(8,128)(2,1)S(1)} %constant_dynamic-update-slice_fusion.kv_ref) | copy-start | bytes 393220
  10.5 63.4 %all-gather.4.cloned.1.call-start = ((), (), s32[]{:S(2)}) async-start(), calls=%async_computation.2 | async-start | bytes 1966080 | tf_op jit(solution)/shard_map/all_gather | solution.py:181
  62.5 10.7 %all-to-all-start = ((bf16[8,32,256]{2,1,0:T(8,128)(2,1)}), bf16[8,32,256]{2,1,0:T(8,128)(2,1)S(1)}, u32[]{:S(2)}, u32[]{:S(2)}) async-start(bf16[8,32,256]{2,1,0:T(8,128)(2,1)} %bitcast.19), calls=%async_computation | async-start | bytes 262144 | tf_op jit(solution)/shard_map/all_to_all | solution.py:206
  73.2 0.7 copy-start.1
Sparse Core Ops, SparseCore 0:
  10.7 43.4 all-gather.5
  55.8 18.0 all-gather.3

commit v2 on v1

--- a/solution.py
+++ b/solution.py
@@ -10,7 +10,6 @@
 HEAD = 64
 KB = 32
 QB = 64
-PAD_ROWS = 16
 MASKED = -1e30
 
 
@@ -26,29 +25,38 @@
     return lax.dot_general(a, b, (((0,), (0,)), ((), ())), preferred_element_type=jnp.float32)
 
 
-def attention_kernel(wanted, q_ref, g_ref, kv_ref, all_ref, sums_ref, bias_ref,
+def pick_kernel(incoming, k_ref, v_ref, out_ref):
+    half = k_ref.shape[1]
+
+    def pick(o, carry):
+        at = pl.ds(pl.multiple_of(jnp.maximum(incoming[o], 0) * KB, KB), KB)
+        out_ref[o, :, :half] = k_ref[at, :]
+        out_ref[o, :, half:] = v_ref[at, :]
+        return carry
+
+    loop(out_ref.shape[0], pick, 0)
+
+
+def loop(count, body, init):
+    if count > 8:
+        return lax.fori_loop(0, count, body, init)
+    for i in range(count):
+        init = body(i, init)
+    return init
+
+
+def attention_kernel(q_ref, g_ref, k_ref, v_ref, kv_sel, sums_ref, bias_ref,
                      dq_ref, own_ref, sel_ref,
-                     kv_sel, dk_own, dv_own, dk_sel, dv_sel, p_buf, dp_buf):
+                     dk_own, dv_own, dk_sel, dv_sel, p_buf, dp_buf):
     span = q_ref.shape[0]
-    half = kv_ref.shape[1] // 2
+    half = k_ref.shape[1]
     kv_local = half // HEAD
     group = q_ref.shape[1] // half
     blocks = span // QB
-    owners = all_ref.shape[0]
+    owners = kv_sel.shape[0] // KB
     scale = HEAD ** -0.5
     chunk = math.gcd(owners, 8) * KB
     chunks = owners * KB // chunk
-
-    def fetch(o, carry):
-        first = pl.multiple_of(jnp.maximum(wanted[o], 0) * KB, KB)
-        kv_sel[pl.ds(pl.multiple_of(o * KB, KB), KB), :] = all_ref[o, pl.ds(first, KB), :]
-        return carry
-
-    if owners <= 8:
-        for o in range(owners):
-            fetch(o, 0)
-    else:
-        lax.fori_loop(0, owners, fetch, 0)
 
     def over_chunks(body, init):
         if chunks == 1:
@@ -69,8 +77,8 @@
             gs = jnp.concatenate([g_ref[rows, i * HEAD:(i + 1) * HEAD] for i in heads], axis=0)
             sums = sums_ref[h * blocks + b:h * blocks + b + 1, :]
             n_own = (b + 1) * QB
-            k_own = kv_ref[:n_own, k_lanes]
-            v_own = kv_ref[:n_own, v_lanes]
+            k_own = k_ref[:n_own, k_lanes]
+            v_own = v_ref[:n_own, k_lanes]
             p_own = jnp.exp(dot_nt(k_own, qs) * scale - sums)
             last = jnp.where(causal, p_own[b * QB:, :], 0.0)
             p_own = jnp.concatenate([p_own[:b * QB, :], last], axis=0) if b else last
@@ -119,9 +127,10 @@
         axis=1).astype(sel_ref.dtype)
 
 
-def landing_kernel(incoming, own_ref, back_ref, x_ref, dk_ref, dv_ref, part_ref, total):
+def landing_kernel(incoming, sources, own_ref, back_ref, *refs):
+    x_refs = refs[:-4]
+    dk_ref, dv_ref, part_ref, total = refs[-4:]
     half = dk_ref.shape[1]
-    owners = back_ref.shape[0]
     total[...] = own_ref[...]
 
     def land(s, carry):
@@ -129,18 +138,16 @@
         total[at, :] += back_ref[s].astype(jnp.float32)
         return carry
 
-    if owners <= 8:
-        for s in range(owners):
-            land(s, 0)
-    else:
-        lax.fori_loop(0, owners, land, 0)
+    loop(back_ref.shape[0], land, 0)
     dk = total[:, :half].astype(jnp.bfloat16)
     dk_ref[...] = dk
     dv_ref[...] = total[:, half:].astype(jnp.bfloat16)
     width = part_ref.shape[2]
-    part = dot_tn(dk, x_ref[...]).astype(part_ref.dtype)
-    for i in range(owners):
-        part_ref[i] = part[:, i * width:(i + 1) * width]
+    for r, x_ref in enumerate(x_refs):
+        part = dot_tn(dk, x_ref[...]).astype(part_ref.dtype)
+        each = x_ref.shape[1] // width
+        for c in range(each):
+            part_ref[sources[r] * each + c] = part[:, c * width:(c + 1) * width]
 
 
 def sum_kernel(parts_ref, out_ref):
@@ -152,7 +159,6 @@
 
 def per_device(queries, key_vectors, value_vectors, log_sums, out_grad, layer_input, chosen):
     owners = lax.axis_size("kv")
-    me = lax.axis_index("kv")
     span, width = queries.shape
     half = key_vectors.shape[1]
     kv_local = half // HEAD
@@ -171,14 +177,25 @@
     used = jnp.any(matched, axis=1)
     bias = jnp.repeat(jnp.where(used, 0.0, MASKED).T, KB, axis=0)
 
-    paired = jnp.concatenate([key_vectors, value_vectors], axis=1)
-    note_rows = -(-owners // (2 * half * PAD_ROWS)) * PAD_ROWS
-    note = jnp.pad(wanted.astype(bf16), (0, note_rows * 2 * half - owners)).reshape(note_rows, 2 * half)
-    sent = jnp.concatenate([paired, note], axis=0)
-    everyone = lax.all_gather(sent, "kv", axis=0, tiled=False)
-    incoming = lax.dynamic_index_in_dim(
-        everyone[:, span:, :].reshape(owners, -1), me, axis=1, keepdims=False).astype(jnp.int32)
-    full_input = lax.all_gather(layer_input, "tp", axis=1, tiled=True)
+    incoming = lax.all_to_all(wanted[:, None], "kv", split_axis=0, concat_axis=0, tiled=True)[:, 0]
+    tp = lax.axis_size("tp")
+    mine = lax.axis_index("tp")
+    pieces, sources = [], []
+    for d in range(tp // 2):
+        turned = [(t, (t + 2 * d) % tp) for t in range(tp)]
+        pieces.append(lax.ppermute(layer_input, "tp", turned) if d else layer_input)
+        sources.append((mine - 2 * d) % tp)
+    for d in range(tp // 2):
+        pieces.append(lax.ppermute(pieces[d], "tp", [(t, t ^ 1) for t in range(tp)]))
+        sources.append(((mine ^ 1) - 2 * d) % tp)
+    outgoing = pl.pallas_call(
+        pick_kernel,
+        name="pick",
+        out_shape=jax.ShapeDtypeStruct((owners, KB, 2 * half), bf16),
+        in_specs=[smem, vmem, vmem],
+        out_specs=vmem,
+    )(incoming, key_vectors, value_vectors)
+    fetched = lax.all_to_all(outgoing, "kv", split_axis=0, concat_axis=0, tiled=True)
     sums = log_sums.reshape(blocks, QB, kv_local, group).transpose(2, 0, 3, 1).reshape(
         kv_local * blocks, group * QB)
 
@@ -190,10 +207,9 @@
             jax.ShapeDtypeStruct((span, 2 * half), f32),
             jax.ShapeDtypeStruct((owners * KB, 2 * half), bf16),
         ),
-        in_specs=[smem] + [vmem] * 6,
+        in_specs=[vmem] * 7,
         out_specs=(vmem,) * 3,
         scratch_shapes=[
-            pltpu.VMEM((owners * KB, 2 * half), bf16),
             pltpu.VMEM((kv_local, span, HEAD), f32),
             pltpu.VMEM((kv_local, span, HEAD), f32),
             pltpu.VMEM((kv_local, owners * KB, HEAD), f32),
@@ -201,10 +217,10 @@
             pltpu.VMEM((owners * KB, group * QB), f32),
             pltpu.VMEM((owners * KB, group * QB), f32),
         ],
-    )(wanted, queries, out_grad, paired, everyone, sums, bias)
+    )(queries, out_grad, key_vectors, value_vectors, fetched.reshape(owners * KB, 2 * half), sums, bias)
 
     back = lax.all_to_all(sel.reshape(owners, KB, 2 * half), "kv", split_axis=0, concat_axis=0, tiled=True)
-    rows = full_input.shape[1] // owners
+    rows = layer_input.shape[1] * tp // owners
     key_grad, value_grad, parts = pl.pallas_call(
         landing_kernel,
         name="landing",
@@ -213,10 +229,10 @@
             jax.ShapeDtypeStruct((span, half), bf16),
             jax.ShapeDtypeStruct((owners, half, rows), bf16),
         ),
-        in_specs=[smem] + [vmem] * 3,
+        in_specs=[smem] * 2 + [vmem] * (2 + tp),
         out_specs=(vmem,) * 3,
         scratch_shapes=[pltpu.VMEM((span, 2 * half), f32)],
-    )(incoming, own, back, full_input)
+    )(incoming, jnp.stack(sources), own, back, *pieces)
     parts = lax.all_to_all(parts, "kv", split_axis=0, concat_axis=0, tiled=True)
     weight_grad = pl.pallas_call(
         sum_kernel,

time: 112 us -> 76.2 us (0.68)
  waiting for transfers between devices: 48 us -> 19.2 us
  between operations: 14.1 us -> 0.77 us
  starting transfers between devices: 3.45 us -> 15.8 us
  blocking collectives: 26.1 us -> 20.6 us
  local copies, waits for them, and re-layouts: 5.3 us -> 2.99 us
  Pallas kernels: 12.5 us -> 13.8 us
    all_gather x2 -> x0, waiting for transfers between devices: 42 us -> none  [the longest x1 41.2 us: per_device(): everyone = lax.all_gather(sent, 'kv', axis=0, tiled=False)]
    all_to_all x0 -> x2, waiting for transfers between devices: none -> 12.6 us  [the longest x1 6.41 us: per_device(): lax.all_to_all(wanted[:, None], 'kv', split_axis=0, concat_axis=0, tiled=...]
    all_to_all x0 -> x2, starting transfers between devices: none -> 9.34 us  [the longest x1 5.83 us: per_device(): lax.all_to_all(wanted[:, None], 'kv', split_axis=0, concat_axis=0, tiled=...]
    all_to_all x1, blocking collectives: 26.1 us -> 20.6 us  [per_device(): parts = lax.all_to_all(parts, 'kv', split_axis=0, concat_axis=0, tiled=True)]
    ppermute x0 -> x3, starting transfers between devices: none -> 3.11 us  [the longest x1 3.03 us: per_device(): pieces.append(lax.ppermute(layer_input, 'tp', turned) if d else layer_input)]
    pallas_call x0 -> x1, Pallas kernels: none -> 1.57 us  [per_device(): pl.pallas_call(pick_kernel, name='pick', out_shape=jax.ShapeDtypeStruct((...]
    all_to_all x1, waiting for transfers between devices: 5.33 us -> 6.63 us  [per_device(): lax.all_to_all(sel.reshape(owners, KB, 2 * half), 'kv', split_axis=0, con...]
  transfers between devices with their start and end apart: 3 -> 6, of which waited for: 3 -> 3; matrix products, arithmetic and copies ran while one was open for 4% -> 6% of each run, Pallas kernels for 7% -> 12%
where the time goes in v2:
time: 76.2 us; the launch traced here: 75.6 us
  blocking collectives  20.6 us (27%)
  waiting for transfers between devices  19.2 us (25%)
  starting transfers between devices  15.8 us (21%)
  Pallas kernels  13.8 us (18%)
  local copies, waits for them, and re-layouts  2.99 us (4%)
  other arithmetic  2.38 us (3%)
  between operations  0.77 us (1%)
    all_to_all x1, blocking collectives, per_device(): parts = lax.all_to_all(parts, 'kv', split_axis=0, concat_axis=0, tiled=True)  20.6 us
    pallas_call x1, Pallas kernels, per_device(): pl.pallas_call(attention_kernel, name='attention', out_shape=(jax.ShapeDt...  7.35 us
    all_to_all x1, waiting for transfers between devices, per_device(): lax.all_to_all(sel.reshape(owners, KB, 2 * half), 'kv', split_axis=0, con...  6.63 us
    all_to_all x1, waiting for transfers between devices, per_device(): lax.all_to_all(wanted[:, None], 'kv', split_axis=0, concat_axis=0, tiled=...  6.41 us
    all_to_all x1, waiting for transfers between devices, per_device(): lax.all_to_all(outgoing, 'kv', split_axis=0, concat_axis=0, tiled=True)  6.18 us
    all_to_all x1, starting transfers between devices, per_device(): lax.all_to_all(wanted[:, None], 'kv', split_axis=0, concat_axis=0, tiled=...  5.83 us
    all_to_all x1, starting transfers between devices, per_device(): lax.all_to_all(outgoing, 'kv', split_axis=0, concat_axis=0, tiled=True)  3.5 us
    all_to_all x1, starting transfers between devices, per_device(): lax.all_to_all(sel.reshape(owners, KB, 2 * half), 'kv', split_axis=0, con...  3.37 us
  transfers between devices with their start and end apart: 6, of which 3 were waited for; matrix products, arithmetic and copies ran while one was open for 6% of the time, Pallas kernels for 12%

profile of v2, /device:TPU:0, one launch (start us, length us, event | category | flops | bytes accessed | tf_op | source)
XLA Modules:
  0.0 75.6 jit_solution(376197609062054544)
XLA Ops:
  0.6 3.0 %collective-permute-start = (bf16[256,768]{1,0:T(8,128)(2,1)}, bf16[256,768]{1,0:T(8,128)(2,1)S(1)}, u32[]{:S(2)}, u32[]{:S(2)}) collective-permute-start(bf16[256,768]{1,0:T(8,128)(2,1)} %refs_0_.1), channel_id=1, source_target_pairs={{0,2},{1,3},{2,0},{3,1},{4,6},{5,7},{6,4},{7,5},{8,10},{9,11},{10,... | collective-permute-start | bytes 1179656 | tf_op jit(solution)/shard_map/ppermute | solution.py:186
  3.7 0.7 fusion.1
  4.4 0.1 select_reduce_fusion
  4.5 0.7 copy.17
  5.2 5.8 %all-to-all-start = ((s32[8,1,1]{2,1,0:T(1,128)}), s32[8,1,1]{2,1,0:T(1,128)S(1)}, u32[]{:S(2)}, u32[]{:S(2)}) async-start(s32[8,1,1]{2,1,0:T(1,128)} %copy.17), calls=%async_computation | async-start | bytes 8192 | tf_op jit(solution)/shard_map/all_to_all | solution.py:180
  11.0 0.0 collective-permute-start.1
  11.0 6.4 %all-to-all-done = s32[8,1,1]{2,1,0:T(1,128)S(1)} async-done(((s32[8,1,1]{2,1,0:T(1,128)}), s32[8,1,1]{2,1,0:T(1,128)S(1)}, u32[]{:S(2)}, u32[]{:S(2)}) %all-to-all-start) | async-done | bytes 64 | tf_op jit(solution)/shard_map/all_to_all | solution.py:180
  17.4 0.8 %reduce.incoming = s32[8]{0:T(128)} reduce(s32[8,1,1]{2,1,0:T(1,128)S(1)} %all-to-all-done, s32[]{:T(128)} %constant.57.clone.1), dimensions={1,2}, to_apply=%all_to_all.16.reduce_sub_computation | reduce | bytes 68 | tf_op jit(solution)/shard_map/all_to_all | solution.py:180
  18.2 1.6 %pick.1 = bf16[8,32,256]{2,1,0:T(8,128)(2,1)} custom-call(s32[8]{0:T(128)} %reduce.incoming, bf16[256,128]{1,0:T(8,128)(2,1)} %k_ref.3, bf16[256,128]{1,0:T(8,128)(2,1)} %v_ref.3), custom_call_target="tpu_custom_call" | custom-call | tf_op jit(solution)/shard_map/pick/pallas_call | solution.py:191
  19.8 0.0 copy-start.5
  19.8 3.5 %all-to-all-start.1 = ((bf16[8,32,256]{2,1,0:T(8,128)(2,1)}), bf16[8,32,256]{2,1,0:T(8,128)(2,1)S(1)}, u32[]{:S(2)}, u32[]{:S(2)}) async-start(bf16[8,32,256]{2,1,0:T(8,128)(2,1)} %pick.1), calls=%async_computation.1 | async-start | bytes 262144 | tf_op jit(solution)/shard_map/all_to_all | solution.py:198
  23.3 0.1 fusion
  23.5 0.0 collective-permute-done.refs_1_
  23.5 0.0 copy-start.2
  23.5 0.1 collective-permute-start.2
  23.6 0.1 copy.19
  23.7 0.0 copy-done.5
  23.7 0.1 reshape.30
  23.7 0.7 reshape.31.sums_ref
  24.4 6.2 %all-to-all-done.1 = bf16[8,32,256]{2,1,0:T(8,128)(2,1)S(1)} async-done(((bf16[8,32,256]{2,1,0:T(8,128)(2,1)}), bf16[8,32,256]{2,1,0:T(8,128)(2,1)S(1)}, u32[]{:S(2)}, u32[]{:S(2)}) %all-to-all-start.1) | async-done | bytes 131104 | tf_op jit(solution)/shard_map/all_to_all | solution.py:198
  30.6 0.0 copy-start.1
  30.6 0.7 broadcast_in_dim.33
  31.3 0.0 copy-done.1
  31.3 7.3 %attention.1 = (bf16[256,768]{1,0:T(8,128)(2,1)}, f32[256,256]{1,0:T(8,128)}, bf16[256,256]{1,0:T(8,128)(2,1)}) custom-call(bf16[256,768]{1,0:T(8,128)(2,1)} %q_ref.1, bf16[256,768]{1,0:T(8,128)(2,1)} %g_ref.1, bf16[256,128]{1,0:T(8,128)(2,1)} %k_ref.3, bf16[256,128]{1,0:T(8,128)(2,1)} %v_ref.3, bf16[256,256]{1,0:T(8,128)(2,1)} %bitcast.15, ...), custom_call_target="tpu_custom_call" | custom-call | tf_op jit(solution)/shard_map/attention/pallas_call | solution.py:202
  38.6 3.4 %all-to-all-start.2 = ((bf16[8,32,256]{2,1,0:T(8,128)(2,1)}), bf16[8,32,256]{2,1,0:T(8,128)(2,1)S(1)}, u32[]{:S(2)}, u32[]{:S(2)}) async-start(bf16[8,32,256]{2,1,0:T(8,128)(2,1)} %bitcast.18), calls=%async_computation.2 | async-start | bytes 262144 | tf_op jit(solution)/shard_map/all_to_all | solution.py:222
  42.1 0.6 pad_add_fusion.sources
  42.7 0.0 collective-permute-done.1.refs_2_
  42.7 0.0 copy-start.3
  42.7 6.6 %all-to-all-done.2.back_ref = bf16[8,32,256]{2,1,0:T(8,128)(2,1)S(1)} async-done(((bf16[8,32,256]{2,1,0:T(8,128)(2,1)}), bf16[8,32,256]{2,1,0:T(8,128)(2,1)S(1)}, u32[]{:S(2)}, u32[]{:S(2)}) %all-to-all-start.2) | async-done | bytes 131104 | tf_op jit(solution)/shard_map/all_to_all | solution.py:222
  49.3 0.0 copy-start
  49.3 0.0 collective-permute-done.2.refs_3_
  49.3 0.0 copy-start.4
  49.3 0.0 copy-done.2
  49.3 0.0 copy-done.3
  49.3 0.6 copy-done
  50.0 0.1 copy-done.4
  50.1 2.9 %landing.1 = (bf16[256,128]{1,0:T(8,128)(2,1)}, bf16[256,128]{1,0:T(8,128)(2,1)}, bf16[8,128,384]{2,1,0:T(8,128)(2,1)}) custom-call(s32[8]{0:T(128)} %reduce.incoming, s32[4]{0:T(128)} %pad_add_fusion.sources, f32[256,256]{1,0:T(8,128)} %get-tuple-element.11.own_ref, bf16[8,32,256]{2,1,0:T(8,128)(2,1)} %copy-done, bf16[256,768]{1,0:T(8,128)(2,1)} %refs_0_.1, ...), custom_call_target="tpu_custom_call" | custom-call | tf_op jit(solution)/shard_map/landing/pallas_call | solution.py:224
  53.0 20.6 %all_to_all.24.parts_ref = bf16[8,128,384]{2,1,0:T(8,128)(2,1)} all-to-all(bf16[8,128,384]{2,1,0:T(8,128)(2,1)} %get-tuple-element.15), channel_id=1, replica_groups=mesh['kv'=8,'tp'=4] {'kv'}, dimensions={0} | all-to-all | bytes 1572864 | tf_op jit(solution)/shard_map/all_to_all | solution.py:236
  73.6 2.0 %sum_parts.1 = f32[384,128]{1,0:T(8,128)} custom-call(bf16[8,128,384]{2,1,0:T(8,128)(2,1)} %all_to_all.24.parts_ref), custom_call_target="tpu_custom_call" | custom-call | tf_op jit(solution)/shard_map/sum_parts/pallas_call | solution.py:237
  (2 shorter events, 0.0 us)
Async XLA Ops:
  0.6 22.8 %collective-permute-start = (bf16[256,768]{1,0:T(8,128)(2,1)}, bf16[256,768]{1,0:T(8,128)(2,1)S(1)}, u32[]{:S(2)}, u32[]{:S(2)}) collective-permute-start(bf16[256,768]{1,0:T(8,128)(2,1)} %refs_0_.1), channel_id=1, source_target_pairs={{0,2},{1,3},{2,0},{3,1},{4,6},{5,7},{6,4},{7,5},{8,10},{9,11},{10,... | collective-permute-start | bytes 1179656 | tf_op jit(solution)/shard_map/ppermute | solution.py:186
  5.2 12.3 %all-to-all-start = ((s32[8,1,1]{2,1,0:T(1,128)}), s32[8,1,1]{2,1,0:T(1,128)S(1)}, u32[]{:S(2)}, u32[]{:S(2)}) async-start(s32[8,1,1]{2,1,0:T(1,128)} %copy.17), calls=%async_computation | async-start | bytes 8192 | tf_op jit(solution)/shard_map/all_to_all | solution.py:180
  11.0 31.7 %collective-permute-start.1 = (bf16[256,768]{1,0:T(8,128)(2,1)}, bf16[256,768]{1,0:T(8,128)(2,1)S(1)}, u32[]{:S(2)}, u32[]{:S(2)}) collective-permute-start(bf16[256,768]{1,0:T(8,128)(2,1)} %refs_0_.1), channel_id=1, source_target_pairs={{0,1},{1,0},{2,3},{3,2},{4,5},{5,4},{6,7},{7,6},{8,9},{9,8},{10,11... | collective-permute-start | bytes 1179656 | tf_op jit(solution)/shard_map/ppermute | solution.py:189
  19.8 3.9 %copy-start.5 = (f32[256,12]{0,1:T(8,128)S(1)}, f32[256,12]{0,1:T(8,128)}, u32[]{:S(2)}) copy-start(f32[256,12]{0,1:T(8,128)} %param.10) | copy-start | bytes 36868
  19.8 10.8 %all-to-all-start.1 = ((bf16[8,32,256]{2,1,0:T(8,128)(2,1)}), bf16[8,32,256]{2,1,0:T(8,128)(2,1)S(1)}, u32[]{:S(2)}, u32[]{:S(2)}) async-start(bf16[8,32,256]{2,1,0:T(8,128)(2,1)} %pick.1), calls=%async_computation.1 | async-start | bytes 262144 | tf_op jit(solution)/shard_map/all_to_all | solution.py:198
  23.5 25.8 %copy-start.2 = (bf16[256,768]{1,0:T(8,128)(2,1)}, bf16[256,768]{1,0:T(8,128)(2,1)S(1)}, u32[]{:S(2)}) copy-start(bf16[256,768]{1,0:T(8,128)(2,1)S(1)} %collective-permute-done.refs_1_) | copy-start | bytes 1179652
  23.5 25.8 %collective-permute-start.2 = (bf16[256,768]{1,0:T(8,128)(2,1)S(1)}, bf16[256,768]{1,0:T(8,128)(2,1)S(1)}, u32[]{:S(2)}, u32[]{:S(2)}) collective-permute-start(bf16[256,768]{1,0:T(8,128)(2,1)S(1)} %collective-permute-done.refs_1_), channel_id=1, source_target_pairs={{0,1},{1,0},{2,3},{3,2},{4,5},{5,4},{6,7},{7,6},{8,9},{9,8},{10,11... | collective-permute-start | bytes 1179656 | tf_op jit(solution)/shard_map/ppermute | solution.py:189
  30.6 0.7 copy-start.1
  38.6 10.7 %all-to-all-start.2 = ((bf16[8,32,256]{2,1,0:T(8,128)(2,1)}), bf16[8,32,256]{2,1,0:T(8,128)(2,1)S(1)}, u32[]{:S(2)}, u32[]{:S(2)}) async-start(bf16[8,32,256]{2,1,0:T(8,128)(2,1)} %bitcast.18), calls=%async_computation.2 | async-start | bytes 262144 | tf_op jit(solution)/shard_map/all_to_all | solution.py:222
  42.7 6.7 %copy-start.3 = (bf16[256,768]{1,0:T(8,128)(2,1)}, bf16[256,768]{1,0:T(8,128)(2,1)S(1)}, u32[]{:S(2)}) copy-start(bf16[256,768]{1,0:T(8,128)(2,1)S(1)} %collective-permute-done.1.refs_2_) | copy-start | bytes 1179652
  49.3 0.7 copy-start
  49.3 0.8 %copy-start.4 = (bf16[256,768]{1,0:T(8,128)(2,1)}, bf16[256,768]{1,0:T(8,128)(2,1)S(1)}, u32[]{:S(2)}) copy-start(bf16[256,768]{1,0:T(8,128)(2,1)S(1)} %collective-permute-done.2.refs_3_) | copy-start | bytes 1179652

commit v3 on v2

--- a/solution.py
+++ b/solution.py
@@ -25,11 +25,30 @@
     return lax.dot_general(a, b, (((0,), (0,)), ((), ())), preferred_element_type=jnp.float32)
 
 
+def table_kernel(chosen, wanted_ref, bias_ref):
+    row = lax.broadcasted_iota(jnp.int32, wanted_ref.shape, 0)
+    lane = lax.broadcasted_iota(jnp.int32, wanted_ref.shape, 1)
+    blocks, entries = chosen.shape
+    per_owner = blocks * QB // KB
+    wanted = jnp.full(wanted_ref.shape, -1, jnp.int32)
+    bias = jnp.full(wanted_ref.shape, MASKED, jnp.float32)
+    for b in range(blocks):
+        for j in range(entries):
+            c = chosen[b, j]
+            at_zero = jnp.maximum(c, 0)
+            owner = jnp.where(c >= 0, at_zero // per_owner, -1)
+            hit = row == owner
+            wanted = jnp.where(hit, at_zero % per_owner, wanted)
+            bias = jnp.where(hit & (lane == b), 0.0, bias)
+    wanted_ref[...] = wanted
+    bias_ref[...] = bias
+
+
 def pick_kernel(incoming, k_ref, v_ref, out_ref):
     half = k_ref.shape[1]
 
     def pick(o, carry):
-        at = pl.ds(pl.multiple_of(jnp.maximum(incoming[o], 0) * KB, KB), KB)
+        at = pl.ds(pl.multiple_of(jnp.maximum(incoming[o, 0], 0) * KB, KB), KB)
         out_ref[o, :, :half] = k_ref[at, :]
         out_ref[o, :, half:] = v_ref[at, :]
         return carry
@@ -45,7 +64,7 @@
     return init
 
 
-def attention_kernel(q_ref, g_ref, k_ref, v_ref, kv_sel, sums_ref, bias_ref,
+def attention_kernel(bias, q_ref, g_ref, k_ref, v_ref, kv_sel, sums_ref,
                      dq_ref, own_ref, sel_ref,
                      dk_own, dv_own, dk_sel, dv_sel, p_buf, dp_buf):
     span = q_ref.shape[0]
@@ -73,13 +92,13 @@
         for b in range(blocks):
             rows = slice(b * QB, (b + 1) * QB)
             heads = [h * group + i for i in range(group)]
-            qs = jnp.concatenate([q_ref[rows, i * HEAD:(i + 1) * HEAD] for i in heads], axis=0)
+            qs = jnp.concatenate([q_ref[rows, i * HEAD:(i + 1) * HEAD] for i in heads], axis=0) * jnp.bfloat16(scale)
             gs = jnp.concatenate([g_ref[rows, i * HEAD:(i + 1) * HEAD] for i in heads], axis=0)
             sums = sums_ref[h * blocks + b:h * blocks + b + 1, :]
             n_own = (b + 1) * QB
             k_own = k_ref[:n_own, k_lanes]
             v_own = v_ref[:n_own, k_lanes]
-            p_own = jnp.exp(dot_nt(k_own, qs) * scale - sums)
+            p_own = jnp.exp(dot_nt(k_own, qs) - sums)
             last = jnp.where(causal, p_own[b * QB:, :], 0.0)
             p_own = jnp.concatenate([p_own[:b * QB, :], last], axis=0) if b else last
             dp_own = dot_nt(v_own, gs)
@@ -88,8 +107,10 @@
 
             def first_pass(c, delta):
                 at = pl.ds(c * chunk, chunk)
-                s = dot_nt(kv_sel[at, k_lanes], qs) * scale - sums
-                p = jnp.exp(s + bias_ref[at, b:b + 1])
+                s = dot_nt(kv_sel[at, k_lanes], qs)
+                p = jnp.exp(jnp.concatenate(
+                    [s[i * KB:(i + 1) * KB] + (bias[c * (chunk // KB) + i, b] - sums)
+                     for i in range(chunk // KB)], axis=0))
                 dp = dot_nt(kv_sel[at, v_lanes], gs)
                 p_buf[at, :] = p
                 dp_buf[at, :] = dp
@@ -121,9 +142,9 @@
             dq = jnp.concatenate([dq[i * QB:(i + 1) * QB] for i in range(group)], axis=1)
             dq_ref[rows, h * group * HEAD:(h + 1) * group * HEAD] = dq.astype(jnp.bfloat16)
     own_ref[...] = jnp.concatenate(
-        [dk_own[h] * scale for h in range(kv_local)] + [dv_own[h] for h in range(kv_local)], axis=1)
+        [dk_own[h] for h in range(kv_local)] + [dv_own[h] for h in range(kv_local)], axis=1)
     sel_ref[...] = jnp.concatenate(
-        [dk_sel[h] * scale for h in range(kv_local)] + [dv_sel[h] for h in range(kv_local)],
+        [dk_sel[h] for h in range(kv_local)] + [dv_sel[h] for h in range(kv_local)],
         axis=1).astype(sel_ref.dtype)
 
 
@@ -134,7 +155,7 @@
     total[...] = own_ref[...]
 
     def land(s, carry):
-        at = pl.ds(pl.multiple_of(jnp.maximum(incoming[s], 0) * KB, KB), KB)
+        at = pl.ds(pl.multiple_of(jnp.maximum(incoming[s, 0], 0) * KB, KB), KB)
         total[at, :] += back_ref[s].astype(jnp.float32)
         return carry
 
@@ -164,20 +185,19 @@
     kv_local = half // HEAD
     group = width // half
     blocks = span // QB
-    blocks_here = span // KB
     f32, bf16 = jnp.float32, jnp.bfloat16
     vmem = pl.BlockSpec(memory_space=pltpu.VMEM)
     smem = pl.BlockSpec(memory_space=pltpu.SMEM)
 
-    ids = jnp.arange(owners, dtype=jnp.int32)
-    owner_of = jnp.where(chosen >= 0, chosen // blocks_here, -1)
-    matched = owner_of[:, :, None] == ids[None, None, :]
-    within = (chosen % blocks_here)[:, :, None]
-    wanted = jnp.max(jnp.where(matched, within, -1), axis=(0, 1))
-    used = jnp.any(matched, axis=1)
-    bias = jnp.repeat(jnp.where(used, 0.0, MASKED).T, KB, axis=0)
-
-    incoming = lax.all_to_all(wanted[:, None], "kv", split_axis=0, concat_axis=0, tiled=True)[:, 0]
+    wanted, bias = pl.pallas_call(
+        table_kernel,
+        name="tables",
+        out_shape=(jax.ShapeDtypeStruct((owners, 128), jnp.int32),
+                   jax.ShapeDtypeStruct((owners, 128), f32)),
+        in_specs=[smem],
+        out_specs=(vmem, vmem),
+    )(chosen)
+    incoming = lax.all_to_all(wanted, "kv", split_axis=0, concat_axis=0, tiled=True)
     tp = lax.axis_size("tp")
     mine = lax.axis_index("tp")
     pieces, sources = [], []
@@ -207,7 +227,7 @@
             jax.ShapeDtypeStruct((span, 2 * half), f32),
             jax.ShapeDtypeStruct((owners * KB, 2 * half), bf16),
         ),
-        in_specs=[vmem] * 7,
+        in_specs=[smem] + [vmem] * 6,
         out_specs=(vmem,) * 3,
         scratch_shapes=[
             pltpu.VMEM((kv_local, span, HEAD), f32),
@@ -217,7 +237,7 @@
             pltpu.VMEM((owners * KB, group * QB), f32),
             pltpu.VMEM((owners * KB, group * QB), f32),
         ],
-    )(queries, out_grad, key_vectors, value_vectors, fetched.reshape(owners * KB, 2 * half), sums, bias)
+    )(bias, queries, out_grad, key_vectors, value_vectors, fetched.reshape(owners * KB, 2 * half), sums)
 
     back = lax.all_to_all(sel.reshape(owners, KB, 2 * half), "kv", split_axis=0, concat_axis=0, tiled=True)
     rows = layer_input.shape[1] * tp // owners
@@ -234,12 +254,14 @@
         scratch_shapes=[pltpu.VMEM((span, 2 * half), f32)],
     )(incoming, jnp.stack(sources), own, back, *pieces)
     parts = lax.all_to_all(parts, "kv", split_axis=0, concat_axis=0, tiled=True)
+    step = 128 if rows % 128 == 0 else rows
     weight_grad = pl.pallas_call(
         sum_kernel,
         name="sum_parts",
         out_shape=jax.ShapeDtypeStruct((rows, half), f32),
-        in_specs=[vmem],
-        out_specs=vmem,
+        grid=(rows // step,),
+        in_specs=[pl.BlockSpec((owners, half, step), lambda i: (0, 0, i))],
+        out_specs=pl.BlockSpec((step, half), lambda i: (i, 0)),
     )(parts)
     return (query_grad, key_grad, value_grad, weight_grad)
 

time: 76.2 us -> 76 us (level)
  blocking collectives: 20.6 us -> 32.8 us
  waiting for transfers between devices: 19.2 us -> 12.5 us
  starting transfers between devices: 15.8 us -> 10.5 us
  Pallas kernels: 13.8 us -> 16 us
  other arithmetic: 2.38 us -> 0.61 us
  local copies, waits for them, and re-layouts: 2.99 us -> 2.21 us
    all_to_all x0 -> x1, blocking collectives: none -> 12.4 us  [per_device(): lax.all_to_all(wanted, 'kv', split_axis=0, concat_axis=0, tiled=True)]
    all_to_all x1 -> x0, waiting for transfers between devices: 6.41 us -> none  [per_device(): lax.all_to_all(wanted[:, None], 'kv', split_axis=0, concat_axis=0, tiled=...]
    all_to_all x1 -> x0, starting transfers between devices: 5.83 us -> none  [per_device(): lax.all_to_all(wanted[:, None], 'kv', split_axis=0, concat_axis=0, tiled=...]
    pallas_call x0 -> x1, Pallas kernels: none -> 1.54 us  [per_device(): pl.pallas_call(table_kernel, name='tables', out_shape=(jax.ShapeDtypeStru...]
    all_to_all x1 -> x0, other arithmetic: 0.83 us -> none  [per_device(): lax.all_to_all(wanted[:, None], 'kv', split_axis=0, concat_axis=0, tiled=...]
    pallas_call x1, Pallas kernels: 1.98 us -> 2.77 us  [per_device(): pl.pallas_call(sum_kernel, name='sum_parts', out_shape=jax.ShapeDtypeStru...]
  transfers between devices with their start and end apart: 6 -> 5, of which waited for: 3 -> 2; matrix products, arithmetic and copies ran while one was open for 6% -> 2% of each run, Pallas kernels for 12% -> 14%
where the time goes in v3:
time: 76 us; the launch traced here: 75.4 us
  blocking collectives  32.8 us (43%)
  Pallas kernels  16 us (21%)
  waiting for transfers between devices  12.5 us (16%)
  starting transfers between devices  10.5 us (14%)
  local copies, waits for them, and re-layouts  2.21 us (3%)
  between operations  0.77 us (1%)
    all_to_all x1, blocking collectives, per_device(): parts = lax.all_to_all(parts, 'kv', split_axis=0, concat_axis=0, tiled=True)  20.4 us
    all_to_all x1, blocking collectives, per_device(): lax.all_to_all(wanted, 'kv', split_axis=0, concat_axis=0, tiled=True)  12.4 us
    pallas_call x1, Pallas kernels, per_device(): pl.pallas_call(attention_kernel, name='attention', out_shape=(jax.ShapeDt...  7.23 us
    all_to_all x1, waiting for transfers between devices, per_device(): lax.all_to_all(sel.reshape(owners, KB, 2 * half), 'kv', split_axis=0, con...  6.6 us
    all_to_all x1, waiting for transfers between devices, per_device(): lax.all_to_all(outgoing, 'kv', split_axis=0, concat_axis=0, tiled=True)  5.92 us
    all_to_all x1, starting transfers between devices, per_device(): lax.all_to_all(outgoing, 'kv', split_axis=0, concat_axis=0, tiled=True)  3.5 us
    all_to_all x1, starting transfers between devices, per_device(): lax.all_to_all(sel.reshape(owners, KB, 2 * half), 'kv', split_axis=0, con...  3.37 us
    ppermute x1, starting transfers between devices, per_device(): pieces.append(lax.ppermute(layer_input, 'tp', turned) if d else layer_input)  3.03 us
  transfers between devices with their start and end apart: 5, of which 2 were waited for; matrix products, arithmetic and copies ran while one was open for 2% of the time, Pallas kernels for 14%

profile of v3, /device:TPU:0, one launch (start us, length us, event | category | flops | bytes accessed | tf_op | source)
XLA Modules:
  0.0 75.4 jit_solution(9896233164713967210)
XLA Ops:
  0.6 0.0 copy-start.2
  0.6 3.0 %collective-permute-start = (bf16[256,768]{1,0:T(8,128)(2,1)}, bf16[256,768]{1,0:T(8,128)(2,1)S(1)}, u32[]{:S(2)}, u32[]{:S(2)}) collective-permute-start(bf16[256,768]{1,0:T(8,128)(2,1)} %refs_0_.1), channel_id=1, source_target_pairs={{0,2},{1,3},{2,0},{3,1},{4,6},{5,7},{6,4},{7,5},{8,10},{9,11},{10,... | collective-permute-start | bytes 1179656 | tf_op jit(solution)/shard_map/ppermute | solution.py:206
  3.7 1.5 %tables.1 = (s32[8,128]{1,0:T(8,128)}, f32[8,128]{1,0:T(8,128)}) custom-call(s32[4,16]{1,0:T(4,128)} %chosen.1), custom_call_target="tpu_custom_call" | custom-call | tf_op jit(solution)/shard_map/tables/pallas_call | solution.py:192
  5.2 12.4 %all_to_all.26 = s32[8,1,128]{2,1,0:T(1,128)} all-to-all(s32[8,1,128]{2,1,0:T(1,128)} %bitcast.20), channel_id=1, replica_groups=mesh['kv'=8,'tp'=4] {'kv'}, dimensions={0} | all-to-all | bytes 8192 | tf_op jit(solution)/shard_map/all_to_all | solution.py:200
  17.6 1.6 %pick.1 = bf16[8,32,256]{2,1,0:T(8,128)(2,1)} custom-call(s32[8,128]{1,0:T(8,128)} %bitcast.18, bf16[256,128]{1,0:T(8,128)(2,1)} %k_ref.3, bf16[256,128]{1,0:T(8,128)(2,1)} %v_ref.3), custom_call_target="tpu_custom_call" | custom-call | tf_op jit(solution)/shard_map/pick/pallas_call | solution.py:211
  19.1 0.0 copy-start.6
  19.1 3.5 %all-to-all-start.1 = ((bf16[8,32,256]{2,1,0:T(8,128)(2,1)}), bf16[8,32,256]{2,1,0:T(8,128)(2,1)S(1)}, u32[]{:S(2)}, u32[]{:S(2)}) async-start(bf16[8,32,256]{2,1,0:T(8,128)(2,1)} %pick.1), calls=%async_computation.1 | async-start | bytes 262144 | tf_op jit(solution)/shard_map/all_to_all | solution.py:218
  22.7 0.0 copy-done.2
  22.7 0.1 collective-permute-start.1
  22.7 0.0 collective-permute-done.refs_1_
  22.8 0.0 copy-start.3
  22.8 0.5 collective-permute-start.2
  23.2 0.0 copy-done.6
  23.3 0.1 reshape.23
  23.3 0.7 reshape.24.sums_ref
  24.0 5.9 %all-to-all-done.1 = bf16[8,32,256]{2,1,0:T(8,128)(2,1)S(1)} async-done(((bf16[8,32,256]{2,1,0:T(8,128)(2,1)}), bf16[8,32,256]{2,1,0:T(8,128)(2,1)S(1)}, u32[]{:S(2)}, u32[]{:S(2)}) %all-to-all-start.1) | async-done | bytes 131104 | tf_op jit(solution)/shard_map/all_to_all | solution.py:218
  29.9 0.0 copy-start.1
  29.9 0.7 copy-done.1
  30.6 7.2 %attention.1 = (bf16[256,768]{1,0:T(8,128)(2,1)}, f32[256,256]{1,0:T(8,128)}, bf16[256,256]{1,0:T(8,128)(2,1)}) custom-call(f32[8,128]{1,0:T(8,128)} %get-tuple-element.12.bias, bf16[256,768]{1,0:T(8,128)(2,1)} %q_ref.1, bf16[256,768]{1,0:T(8,128)(2,1)} %g_ref.1, bf16[256,128]{1,0:T(8,128)(2,1)} %k_ref.3, bf16[256,128]{1,0:T(8,128)(2,1)} %v_ref.3, ...), custom_call_target="tpu_custom_call" | custom-call | tf_op jit(solution)/shard_map/attention/pallas_call | solution.py:222
  37.8 3.4 %all-to-all-start.2 = ((bf16[8,32,256]{2,1,0:T(8,128)(2,1)}), bf16[8,32,256]{2,1,0:T(8,128)(2,1)S(1)}, u32[]{:S(2)}, u32[]{:S(2)}) async-start(bf16[8,32,256]{2,1,0:T(8,128)(2,1)} %bitcast.17), calls=%async_computation.2 | async-start | bytes 262144 | tf_op jit(solution)/shard_map/all_to_all | solution.py:242
  41.3 0.6 pad_add_fusion.sources
  41.9 0.0 collective-permute-done.1.refs_2_
  41.9 0.0 copy-start.4
  41.9 6.6 %all-to-all-done.2.back_ref = bf16[8,32,256]{2,1,0:T(8,128)(2,1)S(1)} async-done(((bf16[8,32,256]{2,1,0:T(8,128)(2,1)}), bf16[8,32,256]{2,1,0:T(8,128)(2,1)S(1)}, u32[]{:S(2)}, u32[]{:S(2)}) %all-to-all-start.2) | async-done | bytes 131104 | tf_op jit(solution)/shard_map/all_to_all | solution.py:242
  48.5 0.0 copy-start
  48.5 0.0 collective-permute-done.2.refs_3_
  48.5 0.0 copy-start.5
  48.5 0.0 copy-done.3
  48.5 0.0 copy-done.4
  48.5 0.6 copy-done
  49.1 0.1 copy-done.5
  49.3 2.9 %landing.1 = (bf16[256,128]{1,0:T(8,128)(2,1)}, bf16[256,128]{1,0:T(8,128)(2,1)}, bf16[8,128,384]{2,1,0:T(8,128)(2,1)}) custom-call(s32[8,128]{1,0:T(8,128)} %bitcast.19, s32[4]{0:T(128)} %pad_add_fusion.sources, f32[256,256]{1,0:T(8,128)} %get-tuple-element.15.own_ref, bf16[8,32,256]{2,1,0:T(8,128)(2,1)} %copy-done, bf16[256,768]{1,0:T(8,128)(2,1)} %refs_0_.1, ...), custom_call_target="tpu_custom_call" | custom-call | tf_op jit(solution)/shard_map/landing/pallas_call | solution.py:244
  52.2 20.4 %all_to_all.27.parts_ref = bf16[8,128,384]{2,1,0:T(8,128)(2,1)} all-to-all(bf16[8,128,384]{2,1,0:T(8,128)(2,1)} %get-tuple-element.19), channel_id=1, replica_groups=mesh['kv'=8,'tp'=4] {'kv'}, dimensions={0} | all-to-all | bytes 1572864 | tf_op jit(solution)/shard_map/all_to_all | solution.py:256
  72.6 2.8 %sum_parts.1 = f32[384,128]{1,0:T(8,128)} custom-call(bf16[8,128,384]{2,1,0:T(8,128)(2,1)} %all_to_all.27.parts_ref), custom_call_target="tpu_custom_call" | custom-call | tf_op jit(solution)/shard_map/sum_parts/pallas_call | solution.py:258
  (1 shorter events, 0.0 us)
Async XLA Ops:
  0.6 22.0 %copy-start.2 = (bf16[256,768]{1,0:T(8,128)(2,1)S(1)}, bf16[256,768]{1,0:T(8,128)(2,1)}, u32[]{:S(2)}) copy-start(bf16[256,768]{1,0:T(8,128)(2,1)} %refs_0_.1) | copy-start | bytes 1179652
  0.6 22.1 %collective-permute-start = (bf16[256,768]{1,0:T(8,128)(2,1)}, bf16[256,768]{1,0:T(8,128)(2,1)S(1)}, u32[]{:S(2)}, u32[]{:S(2)}) collective-permute-start(bf16[256,768]{1,0:T(8,128)(2,1)} %refs_0_.1), channel_id=1, source_target_pairs={{0,2},{1,3},{2,0},{3,1},{4,6},{5,7},{6,4},{7,5},{8,10},{9,11},{10,... | collective-permute-start | bytes 1179656 | tf_op jit(solution)/shard_map/ppermute | solution.py:206
  19.1 4.1 %copy-start.6 = (f32[256,12]{0,1:T(8,128)S(1)}, f32[256,12]{0,1:T(8,128)}, u32[]{:S(2)}) copy-start(f32[256,12]{0,1:T(8,128)} %param.10) | copy-start | bytes 36868
  19.1 10.8 %all-to-all-start.1 = ((bf16[8,32,256]{2,1,0:T(8,128)(2,1)}), bf16[8,32,256]{2,1,0:T(8,128)(2,1)S(1)}, u32[]{:S(2)}, u32[]{:S(2)}) async-start(bf16[8,32,256]{2,1,0:T(8,128)(2,1)} %pick.1), calls=%async_computation.1 | async-start | bytes 262144 | tf_op jit(solution)/shard_map/all_to_all | solution.py:218
  22.7 19.2 %collective-permute-start.1 = (bf16[256,768]{1,0:T(8,128)(2,1)S(1)}, bf16[256,768]{1,0:T(8,128)(2,1)S(1)}, u32[]{:S(2)}, u32[]{:S(2)}) collective-permute-start(bf16[256,768]{1,0:T(8,128)(2,1)S(1)} %copy-done.2), channel_id=1, source_target_pairs={{0,1},{1,0},{2,3},{3,2},{4,5},{5,4},{6,7},{7,6},{8,9},{9,8},{10,11... | collective-permute-start | bytes 1179656 | tf_op jit(solution)/shard_map/ppermute | solution.py:209
  22.8 25.7 %copy-start.3 = (bf16[256,768]{1,0:T(8,128)(2,1)}, bf16[256,768]{1,0:T(8,128)(2,1)S(1)}, u32[]{:S(2)}) copy-start(bf16[256,768]{1,0:T(8,128)(2,1)S(1)} %collective-permute-done.refs_1_) | copy-start | bytes 1179652
  22.8 25.7 %collective-permute-start.2 = (bf16[256,768]{1,0:T(8,128)(2,1)S(1)}, bf16[256,768]{1,0:T(8,128)(2,1)S(1)}, u32[]{:S(2)}, u32[]{:S(2)}) collective-permute-start(bf16[256,768]{1,0:T(8,128)(2,1)S(1)} %collective-permute-done.refs_1_), channel_id=1, source_target_pairs={{0,1},{1,0},{2,3},{3,2},{4,5},{5,4},{6,7},{7,6},{8,9},{9,8},{10,11... | collective-permute-start | bytes 1179656 | tf_op jit(solution)/shard_map/ppermute | solution.py:209
  29.9 0.7 copy-start.1
  37.8 10.7 %all-to-all-start.2 = ((bf16[8,32,256]{2,1,0:T(8,128)(2,1)}), bf16[8,32,256]{2,1,0:T(8,128)(2,1)S(1)}, u32[]{:S(2)}, u32[]{:S(2)}) async-start(bf16[8,32,256]{2,1,0:T(8,128)(2,1)} %bitcast.17), calls=%async_computation.2 | async-start | bytes 262144 | tf_op jit(solution)/shard_map/all_to_all | solution.py:242
  41.9 6.6 %copy-start.4 = (bf16[256,768]{1,0:T(8,128)(2,1)}, bf16[256,768]{1,0:T(8,128)(2,1)S(1)}, u32[]{:S(2)}) copy-start(bf16[256,768]{1,0:T(8,128)(2,1)S(1)} %collective-permute-done.1.refs_2_) | copy-start | bytes 1179652
  48.5 0.7 copy-start
  48.5 0.8 %copy-start.5 = (bf16[256,768]{1,0:T(8,128)(2,1)}, bf16[256,768]{1,0:T(8,128)(2,1)S(1)}, u32[]{:S(2)}) copy-start(bf16[256,768]{1,0:T(8,128)(2,1)S(1)} %collective-permute-done.2.refs_3_) | copy-start | bytes 1179652

commit v4 on v3

--- a/solution.py
+++ b/solution.py
@@ -38,7 +38,8 @@
             at_zero = jnp.maximum(c, 0)
             owner = jnp.where(c >= 0, at_zero // per_owner, -1)
             hit = row == owner
-            wanted = jnp.where(hit, at_zero % per_owner, wanted)
+            seen = row == jnp.where(lane == 1, owner ^ 1, owner)
+            wanted = jnp.where(seen & (c >= 0), at_zero % per_owner, wanted)
             bias = jnp.where(hit & (lane == b), 0.0, bias)
     wanted_ref[...] = wanted
     bias_ref[...] = bias
@@ -65,7 +66,7 @@
 
 
 def attention_kernel(bias, q_ref, g_ref, k_ref, v_ref, kv_sel, sums_ref,
-                     dq_ref, own_ref, sel_ref,
+                     dq_ref, own_ref, own16_ref, sel_ref,
                      dk_own, dv_own, dk_sel, dv_sel, p_buf, dp_buf):
     span = q_ref.shape[0]
     half = k_ref.shape[1]
@@ -143,29 +144,42 @@
             dq_ref[rows, h * group * HEAD:(h + 1) * group * HEAD] = dq.astype(jnp.bfloat16)
     own_ref[...] = jnp.concatenate(
         [dk_own[h] for h in range(kv_local)] + [dv_own[h] for h in range(kv_local)], axis=1)
-    sel_ref[...] = jnp.concatenate(
-        [dk_sel[h] for h in range(kv_local)] + [dv_sel[h] for h in range(kv_local)],
-        axis=1).astype(sel_ref.dtype)
-
-
-def landing_kernel(incoming, sources, own_ref, back_ref, *refs):
+    own16_ref[...] = own_ref[:, :half].astype(own16_ref.dtype)
+
+    def send(o, carry):
+        at = pl.ds(pl.multiple_of(o * KB, KB), KB)
+        dk = jnp.concatenate([dk_sel[h, at, :] for h in range(kv_local)], axis=1).astype(sel_ref.dtype)
+        dv = jnp.concatenate([dv_sel[h, at, :] for h in range(kv_local)], axis=1).astype(sel_ref.dtype)
+        sel_ref[o, :, :half] = dk
+        sel_ref[o, :, half:2 * half] = dv
+        sel_ref[o ^ 1, :, 2 * half:] = dk
+        return carry
+
+    loop(owners, send, 0)
+
+
+def landing_kernel(incoming, sources, own_ref, near_ref, back_ref, *refs):
     x_refs = refs[:-4]
     dk_ref, dv_ref, part_ref, total = refs[-4:]
     half = dk_ref.shape[1]
-    total[...] = own_ref[...]
+    total[:, :2 * half] = own_ref[...]
+    total[:, 2 * half:] = near_ref[...].astype(jnp.float32)
 
     def land(s, carry):
         at = pl.ds(pl.multiple_of(jnp.maximum(incoming[s, 0], 0) * KB, KB), KB)
-        total[at, :] += back_ref[s].astype(jnp.float32)
+        near = pl.ds(pl.multiple_of(jnp.maximum(incoming[s, 1], 0) * KB, KB), KB)
+        total[at, :2 * half] += back_ref[s, :, :2 * half].astype(jnp.float32)
+        total[near, 2 * half:] += back_ref[s, :, 2 * half:].astype(jnp.float32)
         return carry
 
     loop(back_ref.shape[0], land, 0)
     dk = total[:, :half].astype(jnp.bfloat16)
     dk_ref[...] = dk
-    dv_ref[...] = total[:, half:].astype(jnp.bfloat16)
+    dv_ref[...] = total[:, half:2 * half].astype(jnp.bfloat16)
+    both = jnp.concatenate([dk, total[:, 2 * half:].astype(jnp.bfloat16)], axis=0)
     width = part_ref.shape[2]
     for r, x_ref in enumerate(x_refs):
-        part = dot_tn(dk, x_ref[...]).astype(part_ref.dtype)
+        part = dot_tn(both, x_ref[...]).astype(part_ref.dtype)
         each = x_ref.shape[1] // width
         for c in range(each):
             part_ref[sources[r] * each + c] = part[:, c * width:(c + 1) * width]
@@ -200,10 +214,17 @@
     incoming = lax.all_to_all(wanted, "kv", split_axis=0, concat_axis=0, tiled=True)
     tp = lax.axis_size("tp")
     mine = lax.axis_index("tp")
+    parity = lax.axis_index("kv") % 2
+    swap = [(i, i ^ 1) for i in range(owners)]
+    rows = layer_input.shape[1] * tp // owners
+    split = layer_input.reshape(span, -1, 2, rows)
+    kept, given = [lax.dynamic_index_in_dim(split, side, 2, keepdims=False).reshape(span, -1)
+                   for side in (parity, 1 - parity)]
+    pair_input = jnp.concatenate([kept, lax.ppermute(given, "kv", swap)], axis=0)
     pieces, sources = [], []
     for d in range(tp // 2):
         turned = [(t, (t + 2 * d) % tp) for t in range(tp)]
-        pieces.append(lax.ppermute(layer_input, "tp", turned) if d else layer_input)
+        pieces.append(lax.ppermute(pair_input, "tp", turned) if d else pair_input)
         sources.append((mine - 2 * d) % tp)
     for d in range(tp // 2):
         pieces.append(lax.ppermute(pieces[d], "tp", [(t, t ^ 1) for t in range(tp)]))
@@ -219,16 +240,17 @@
     sums = log_sums.reshape(blocks, QB, kv_local, group).transpose(2, 0, 3, 1).reshape(
         kv_local * blocks, group * QB)
 
-    query_grad, own, sel = pl.pallas_call(
+    query_grad, own, own16, sel = pl.pallas_call(
         attention_kernel,
         name="attention",
         out_shape=(
             jax.ShapeDtypeStruct((span, width), bf16),
             jax.ShapeDtypeStruct((span, 2 * half), f32),
-            jax.ShapeDtypeStruct((owners * KB, 2 * half), bf16),
+            jax.ShapeDtypeStruct((span, half), bf16),
+            jax.ShapeDtypeStruct((owners, KB, 3 * half), bf16),
         ),
         in_specs=[smem] + [vmem] * 6,
-        out_specs=(vmem,) * 3,
+        out_specs=(vmem,) * 4,
         scratch_shapes=[
             pltpu.VMEM((kv_local, span, HEAD), f32),
             pltpu.VMEM((kv_local, span, HEAD), f32),
@@ -239,29 +261,29 @@
         ],
     )(bias, queries, out_grad, key_vectors, value_vectors, fetched.reshape(owners * KB, 2 * half), sums)
 
-    back = lax.all_to_all(sel.reshape(owners, KB, 2 * half), "kv", split_axis=0, concat_axis=0, tiled=True)
-    rows = layer_input.shape[1] * tp // owners
+    back = lax.all_to_all(sel, "kv", split_axis=0, concat_axis=0, tiled=True)
+    near = lax.ppermute(own16, "kv", swap)
     key_grad, value_grad, parts = pl.pallas_call(
         landing_kernel,
         name="landing",
         out_shape=(
             jax.ShapeDtypeStruct((span, half), bf16),
             jax.ShapeDtypeStruct((span, half), bf16),
-            jax.ShapeDtypeStruct((owners, half, rows), bf16),
+            jax.ShapeDtypeStruct((owners // 2, half, rows), bf16),
         ),
-        in_specs=[smem] * 2 + [vmem] * (2 + tp),
+        in_specs=[smem] * 2 + [vmem] * (3 + tp),
         out_specs=(vmem,) * 3,
-        scratch_shapes=[pltpu.VMEM((span, 2 * half), f32)],
-    )(incoming, jnp.stack(sources), own, back, *pieces)
-    parts = lax.all_to_all(parts, "kv", split_axis=0, concat_axis=0, tiled=True)
-    step = 128 if rows % 128 == 0 else rows
+        scratch_shapes=[pltpu.VMEM((span, 3 * half), f32)],
+    )(incoming, jnp.stack(sources), own, near, back, *pieces)
+    parity_groups = [list(range(0, owners, 2)), list(range(1, owners, 2))]
+    parts = lax.all_to_all(parts, "kv", split_axis=0, concat_axis=0, tiled=True,
+                           axis_index_groups=parity_groups)
     weight_grad = pl.pallas_call(
         sum_kernel,
         name="sum_parts",
         out_shape=jax.ShapeDtypeStruct((rows, half), f32),
-        grid=(rows // step,),
-        in_specs=[pl.BlockSpec((owners, half, step), lambda i: (0, 0, i))],
-        out_specs=pl.BlockSpec((step, half), lambda i: (i, 0)),
+        in_specs=[vmem],
+        out_specs=vmem,
     )(parts)
     return (query_grad, key_grad, value_grad, weight_grad)
 

time: 76 us -> 77 us (1.013)
  blocking collectives: 32.8 us -> 25.3 us
  starting transfers between devices: 10.5 us -> 14.2 us
  local copies, waits for them, and re-layouts: 2.21 us -> 5.07 us
  waiting for transfers between devices: 12.5 us -> 15.1 us
  Pallas kernels: 16 us -> 15.1 us
    all_to_all x1, blocking collectives: 20.4 us -> 13.1 us  [per_device(): lax.all_to_all(parts, 'kv', split_axis=0, concat_axis=0, tiled=True, axis...]
    ppermute x1 -> x3, waiting for transfers between devices: 0.01 us -> 6.84 us  [the longest x1 4.87 us: per_device(): lax.ppermute(given, 'kv', swap)]
    all_to_all x1, waiting for transfers between devices: 6.6 us -> 2.34 us  [per_device(): back = lax.all_to_all(sel, 'kv', split_axis=0, concat_axis=0, tiled=True)]
    ppermute x1 -> x3, starting transfers between devices: 3.03 us -> 6.75 us  [the longest x1 3.06 us: per_device(): lax.ppermute(given, 'kv', swap)]
    reshape x0 -> x1, local copies, waits for them, and re-layouts: none -> 1.09 us  [per_device(): split = layer_input.reshape(span, -1, 2, rows)]
    unnamed x14 -> x20, local copies, waits for them, and re-layouts: 1.45 us -> 2.41 us
    pallas_call x1, Pallas kernels: 2.77 us -> 1.81 us  [per_device(): pl.pallas_call(sum_kernel, name='sum_parts', out_shape=jax.ShapeDtypeStru...]
    dynamic_slice x0 -> x1, local copies, waits for them, and re-layouts: none -> 0.82 us  [per_device(): lax.dynamic_index_in_dim(split, side, 2, keepdims=False).reshape(span, -1)]
  transfers between devices with their start and end apart: 5 -> 7, of which waited for: 2 -> 4; matrix products, arithmetic and copies ran while one was open for 2% -> 2% of each run, Pallas kernels for 14% -> 14%
where the time goes in v4:
time: 77 us; the launch traced here: 76.3 us
  blocking collectives  25.3 us (33%)
  waiting for transfers between devices  15.1 us (20%)
  Pallas kernels  15.1 us (20%)
  starting transfers between devices  14.2 us (18%)
  local copies, waits for them, and re-layouts  5.07 us (7%)
  between operations  0.84 us (1%)
    all_to_all x1, blocking collectives, per_device(): lax.all_to_all(parts, 'kv', split_axis=0, concat_axis=0, tiled=True, axis...  13.1 us
    all_to_all x1, blocking collectives, per_device(): lax.all_to_all(wanted, 'kv', split_axis=0, concat_axis=0, tiled=True)  12.2 us
    pallas_call x1, Pallas kernels, per_device(): pl.pallas_call(attention_kernel, name='attention', out_shape=(jax.ShapeDt...  7.19 us
    all_to_all x1, waiting for transfers between devices, per_device(): lax.all_to_all(outgoing, 'kv', split_axis=0, concat_axis=0, tiled=True)  5.93 us
    ppermute x1, waiting for transfers between devices, per_device(): lax.ppermute(given, 'kv', swap)  4.87 us
    all_to_all x1, starting transfers between devices, per_device(): lax.all_to_all(outgoing, 'kv', split_axis=0, concat_axis=0, tiled=True)  3.5 us
    all_to_all x1, starting transfers between devices, per_device(): back = lax.all_to_all(sel, 'kv', split_axis=0, concat_axis=0, tiled=True)  3.39 us
    ppermute x1, starting transfers between devices, per_device(): lax.ppermute(given, 'kv', swap)  3.06 us
  transfers between devices with their start and end apart: 7, of which 4 were waited for; matrix products, arithmetic and copies ran while one was open for 2% of the time, Pallas kernels for 14%

profile of v4, /device:TPU:0, one launch (start us, length us, event | category | flops | bytes accessed | tf_op | source)
XLA Modules:
  0.0 76.3 jit_solution(17932954392875708300)
XLA Ops:
  0.6 1.1 %reshape.33 = bf16[256,1,2,384]{3,2,0,1:T(2,128)(2,1)S(1)} reshape(bf16[256,768]{1,0:T(8,128)(2,1)} %param.12) | data formatting | bytes 786432 | tf_op jit(solution)/shard_map/reshape | solution.py:220
  1.8 0.8 %constant_dynamic-slice_fusion.1 = (bf16[256,1,1,384]{3,2,0,1:T(2,128)(2,1)S(1)}, bf16[256,1,1,384]{3,2,0,1:T(2,128)(2,1)S(1)}) fusion(bf16[256,1,2,384]{3,2,0,1:T(2,128)(2,1)S(1)} %reshape.33, s32[]{:T(128)S(6)} %select_n.35, s32[]{:T(128)S(6)} %select_n.36), kind=kLoop, calls=%fused_computation.6 | loop fusion | bytes 786440 | tf_op jit(solution)/shard_map/jit(dynamic_index_in_dim)/dynamic_slice | solution.py:221
  2.6 3.1 %collective-permute-start.1 = (bf16[256,384]{1,0:T(8,128)(2,1)S(1)}, bf16[256,384]{1,0:T(8,128)(2,1)S(1)}, u32[]{:S(2)}, u32[]{:S(2)}) collective-permute-start(bf16[256,384]{1,0:T(8,128)(2,1)S(1)} %bitcast.22), channel_id=1, source_target_pairs={{0,4},{4,0},{8,12},{12,8},{16,20},{20,16},{24,28},{28,24},{1,5},{5... | collective-permute-start | bytes 589832 | tf_op jit(solution)/shard_map/ppermute | solution.py:223
  5.7 4.9 %collective-permute-done.1 = bf16[256,384]{1,0:T(8,128)(2,1)S(1)} collective-permute-done((bf16[256,384]{1,0:T(8,128)(2,1)S(1)}, bf16[256,384]{1,0:T(8,128)(2,1)S(1)}, u32[]{:S(2)}, u32[]{:S(2)}) %collective-permute-start.1) | collective-permute-done | bytes 196640 | tf_op jit(solution)/shard_map/ppermute | solution.py:223
  10.6 0.0 copy-start
  10.6 1.8 %collective-permute-start.2 = (bf16[512,384]{1,0:T(8,128)(2,1)S(1)}, bf16[512,384]{1,0:T(8,128)(2,1)S(1)}, u32[]{:S(2)}, u32[]{:S(2)}) collective-permute-start(bf16[512,384]{1,0:T(8,128)(2,1)S(1)} %pad_maximum_fusion.refs_0_), channel_id=1, source_target_pairs={{0,2},{1,3},{2,0},{3,1},{4,6},{5,7},{6,4},{7,5},{8,10},{9,11},{10,... | collective-permute-start | bytes 1179656 | tf_op jit(solution)/shard_map/ppermute | solution.py:227
  12.4 1.6 %tables.1 = (s32[8,128]{1,0:T(8,128)}, f32[8,128]{1,0:T(8,128)}) custom-call(s32[4,16]{1,0:T(4,128)} %chosen.1), custom_call_target="tpu_custom_call" | custom-call | tf_op jit(solution)/shard_map/tables/pallas_call | solution.py:206
  14.0 12.2 %all_to_all.26 = s32[8,1,128]{2,1,0:T(1,128)} all-to-all(s32[8,1,128]{2,1,0:T(1,128)} %bitcast.26), channel_id=1, replica_groups=mesh['kv'=8,'tp'=4] {'kv'}, dimensions={0} | all-to-all | bytes 8192 | tf_op jit(solution)/shard_map/all_to_all | solution.py:214
  26.2 1.6 %pick.1 = bf16[8,32,256]{2,1,0:T(8,128)(2,1)} custom-call(s32[8,128]{1,0:T(8,128)} %bitcast.24, bf16[256,128]{1,0:T(8,128)(2,1)} %k_ref.3, bf16[256,128]{1,0:T(8,128)(2,1)} %v_ref.3), custom_call_target="tpu_custom_call" | custom-call | tf_op jit(solution)/shard_map/pick/pallas_call | solution.py:232
  27.8 0.0 copy-start.7
  27.8 3.5 %all-to-all-start.1 = ((bf16[8,32,256]{2,1,0:T(8,128)(2,1)}), bf16[8,32,256]{2,1,0:T(8,128)(2,1)S(1)}, u32[]{:S(2)}, u32[]{:S(2)}) async-start(bf16[8,32,256]{2,1,0:T(8,128)(2,1)} %pick.1), calls=%async_computation.1 | async-start | bytes 262144 | tf_op jit(solution)/shard_map/all_to_all | solution.py:239
  31.3 0.1 collective-permute-start.3
  31.4 0.0 collective-permute-done.2.refs_1_
  31.4 0.0 copy-start.3
  31.4 0.5 collective-permute-start.4
  31.9 0.0 copy-done.7
  31.9 0.1 reshape.31
  32.0 0.7 reshape.32.sums_ref
  32.7 5.9 %all-to-all-done.1 = bf16[8,32,256]{2,1,0:T(8,128)(2,1)S(1)} async-done(((bf16[8,32,256]{2,1,0:T(8,128)(2,1)}), bf16[8,32,256]{2,1,0:T(8,128)(2,1)S(1)}, u32[]{:S(2)}, u32[]{:S(2)}) %all-to-all-start.1) | async-done | bytes 131104 | tf_op jit(solution)/shard_map/all_to_all | solution.py:239
  38.6 0.0 copy-start.2
  38.6 0.6 copy-done.2
  39.2 7.2 %attention.1 = (bf16[256,768]{1,0:T(8,128)(2,1)}, f32[256,256]{1,0:T(8,128)}, bf16[256,128]{1,0:T(8,128)(2,1)}, bf16[8,32,384]{2,1,0:T(8,128)(2,1)}) custom-call(f32[8,128]{1,0:T(8,128)} %get-tuple-element.13.bias, bf16[256,768]{1,0:T(8,128)(2,1)} %q_ref.1, bf16[256,768]{1,0:T(8,128)(2,1)} %g_ref.1, bf16[256,128]{1,0:T(8,128)(2,1)} %k_ref.3, ...), custom_call_target="tpu_custom_call" | custom-call | tf_op jit(solution)/shard_map/attention/pallas_call | solution.py:243
  46.4 0.0 copy-done
  46.4 3.4 %all-to-all-start.2 = ((bf16[8,32,384]{2,1,0:T(8,128)(2,1)}), bf16[8,32,384]{2,1,0:T(8,128)(2,1)S(1)}, u32[]{:S(2)}, u32[]{:S(2)}) async-start(bf16[8,32,384]{2,1,0:T(8,128)(2,1)} %get-tuple-element.18), calls=%async_computation.2 | async-start | bytes 393216 | tf_op jit(solution)/shard_map/all_to_all | solution.py:264
  49.8 0.0 copy-start.8
  49.9 0.8 %copy-done.8 = bf16[256,128]{1,0:T(8,128)(2,1)S(1)} copy-done((bf16[256,128]{1,0:T(8,128)(2,1)S(1)}, bf16[256,128]{1,0:T(8,128)(2,1)}, u32[]{:S(2)}) %copy-start.8) | copy-done | bytes 65560
  50.7 1.9 %collective-permute-start = (bf16[256,128]{1,0:T(8,128)(2,1)S(1)}, bf16[256,128]{1,0:T(8,128)(2,1)S(1)}, u32[]{:S(2)}, u32[]{:S(2)}) collective-permute-start(bf16[256,128]{1,0:T(8,128)(2,1)S(1)} %copy-done.8), channel_id=1, source_target_pairs={{0,4},{4,0},{8,12},{12,8},{16,20},{20,16},{24,28},{28,24},{1,5},{5... | collective-permute-start | bytes 196616 | tf_op jit(solution)/shard_map/ppermute | solution.py:265
  52.6 0.6 pad_add_fusion.sources
  53.2 2.0 %collective-permute-done.near_ref = bf16[256,128]{1,0:T(8,128)(2,1)S(1)} collective-permute-done((bf16[256,128]{1,0:T(8,128)(2,1)S(1)}, bf16[256,128]{1,0:T(8,128)(2,1)S(1)}, u32[]{:S(2)}, u32[]{:S(2)}) %collective-permute-start) | collective-permute-done | bytes 65568 | tf_op jit(solution)/shard_map/ppermute | solution.py:265
  55.2 0.0 copy-start.6
  55.2 2.3 %all-to-all-done.2.back_ref = bf16[8,32,384]{2,1,0:T(8,128)(2,1)S(1)} async-done(((bf16[8,32,384]{2,1,0:T(8,128)(2,1)}), bf16[8,32,384]{2,1,0:T(8,128)(2,1)S(1)}, u32[]{:S(2)}, u32[]{:S(2)}) %all-to-all-start.2) | async-done | bytes 196640 | tf_op jit(solution)/shard_map/all_to_all | solution.py:264
  57.6 0.0 copy-start.1
  57.6 0.0 collective-permute-done.3.refs_2_
  57.6 0.0 copy-start.4
  57.6 0.0 collective-permute-done.4.refs_3_
  57.6 0.0 copy-start.5
  57.6 0.0 copy-done.3
  57.6 0.0 copy-done.6
  57.6 0.6 copy-done.1
  58.2 0.1 copy-done.4
  58.4 0.2 copy-done.5
  58.5 2.9 %landing.1 = (bf16[256,128]{1,0:T(8,128)(2,1)}, bf16[256,128]{1,0:T(8,128)(2,1)}, bf16[4,128,384]{2,1,0:T(8,128)(2,1)}) custom-call(s32[8,128]{1,0:T(8,128)} %bitcast.25, s32[4]{0:T(128)} %pad_add_fusion.sources, f32[256,256]{1,0:T(8,128)} %get-tuple-element.16.own_ref, bf16[256,128]{1,0:T(8,128)(2,1)} %copy-done.6, bf16[8,32,384]{2,1,0:T(8,128)(2,1)} %copy-done.1, ...), custom_call_target="tpu_custom_call" | custom-call | tf_op jit(solution)/shard_map/landing/pallas_call | solution.py:266
  61.4 13.1 %all_to_all.27.parts_ref = bf16[4,128,384]{2,1,0:T(8,128)(2,1)} all-to-all(bf16[4,128,384]{2,1,0:T(8,128)(2,1)} %get-tuple-element.21), channel_id=1, replica_groups={{0,8,16,24},{4,12,20,28},{1,9,17,25},{5,13,21,29},{2,10,18,26},{6,14,22..., dimensions={0} | all-to-all | bytes 786432 | tf_op jit(solution)/shard_map/all_to_all | solution.py:279
  74.5 1.8 %sum_parts.1 = f32[384,128]{1,0:T(8,128)} custom-call(bf16[4,128,384]{2,1,0:T(8,128)(2,1)} %all_to_all.27.parts_ref), custom_call_target="tpu_custom_call" | custom-call | tf_op jit(solution)/shard_map/sum_parts/pallas_call | solution.py:281
  (4 shorter events, 0.1 us)
Async XLA Ops:
  2.6 8.0 %collective-permute-start.1 = (bf16[256,384]{1,0:T(8,128)(2,1)S(1)}, bf16[256,384]{1,0:T(8,128)(2,1)S(1)}, u32[]{:S(2)}, u32[]{:S(2)}) collective-permute-start(bf16[256,384]{1,0:T(8,128)(2,1)S(1)} %bitcast.22), channel_id=1, source_target_pairs={{0,4},{4,0},{8,12},{12,8},{16,20},{20,16},{24,28},{28,24},{1,5},{5... | collective-permute-start | bytes 589832 | tf_op jit(solution)/shard_map/ppermute | solution.py:223
  10.6 35.8 %copy-start = (bf16[512,384]{1,0:T(8,128)(2,1)}, bf16[512,384]{1,0:T(8,128)(2,1)S(1)}, u32[]{:S(2)}) copy-start(bf16[512,384]{1,0:T(8,128)(2,1)S(1)} %pad_maximum_fusion.refs_0_) | copy-start | bytes 1179652
  10.6 20.8 %collective-permute-start.2 = (bf16[512,384]{1,0:T(8,128)(2,1)S(1)}, bf16[512,384]{1,0:T(8,128)(2,1)S(1)}, u32[]{:S(2)}, u32[]{:S(2)}) collective-permute-start(bf16[512,384]{1,0:T(8,128)(2,1)S(1)} %pad_maximum_fusion.refs_0_), channel_id=1, source_target_pairs={{0,2},{1,3},{2,0},{3,1},{4,6},{5,7},{6,4},{7,5},{8,10},{9,11},{10,... | collective-permute-start | bytes 1179656 | tf_op jit(solution)/shard_map/ppermute | solution.py:227
  27.8 4.1 %copy-start.7 = (f32[256,12]{0,1:T(8,128)S(1)}, f32[256,12]{0,1:T(8,128)}, u32[]{:S(2)}) copy-start(f32[256,12]{0,1:T(8,128)} %param.10) | copy-start | bytes 36868
  27.8 10.8 %all-to-all-start.1 = ((bf16[8,32,256]{2,1,0:T(8,128)(2,1)}), bf16[8,32,256]{2,1,0:T(8,128)(2,1)S(1)}, u32[]{:S(2)}, u32[]{:S(2)}) async-start(bf16[8,32,256]{2,1,0:T(8,128)(2,1)} %pick.1), calls=%async_computation.1 | async-start | bytes 262144 | tf_op jit(solution)/shard_map/all_to_all | solution.py:239
  31.3 26.2 %collective-permute-start.3 = (bf16[512,384]{1,0:T(8,128)(2,1)S(1)}, bf16[512,384]{1,0:T(8,128)(2,1)S(1)}, u32[]{:S(2)}, u32[]{:S(2)}) collective-permute-start(bf16[512,384]{1,0:T(8,128)(2,1)S(1)} %pad_maximum_fusion.refs_0_), channel_id=1, source_target_pairs={{0,1},{1,0},{2,3},{3,2},{4,5},{5,4},{6,7},{7,6},{8,9},{9,8},{10,11... | collective-permute-start | bytes 1179656 | tf_op jit(solution)/shard_map/ppermute | solution.py:230
  31.4 26.2 %copy-start.3 = (bf16[512,384]{1,0:T(8,128)(2,1)}, bf16[512,384]{1,0:T(8,128)(2,1)S(1)}, u32[]{:S(2)}) copy-start(bf16[512,384]{1,0:T(8,128)(2,1)S(1)} %collective-permute-done.2.refs_1_) | copy-start | bytes 1179652
  31.4 26.1 %collective-permute-start.4 = (bf16[512,384]{1,0:T(8,128)(2,1)S(1)}, bf16[512,384]{1,0:T(8,128)(2,1)S(1)}, u32[]{:S(2)}, u32[]{:S(2)}) collective-permute-start(bf16[512,384]{1,0:T(8,128)(2,1)S(1)} %collective-permute-done.2.refs_1_), channel_id=1, source_target_pairs={{0,1},{1,0},{2,3},{3,2},{4,5},{5,4},{6,7},{7,6},{8,9},{9,8},{10,11... | collective-permute-start | bytes 1179656 | tf_op jit(solution)/shard_map/ppermute | solution.py:230
  38.6 0.6 copy-start.2
  46.4 11.1 %all-to-all-start.2 = ((bf16[8,32,384]{2,1,0:T(8,128)(2,1)}), bf16[8,32,384]{2,1,0:T(8,128)(2,1)S(1)}, u32[]{:S(2)}, u32[]{:S(2)}) async-start(bf16[8,32,384]{2,1,0:T(8,128)(2,1)} %get-tuple-element.18), calls=%async_computation.2 | async-start | bytes 393216 | tf_op jit(solution)/shard_map/all_to_all | solution.py:264
  49.8 0.8 %copy-start.8 = (bf16[256,128]{1,0:T(8,128)(2,1)S(1)}, bf16[256,128]{1,0:T(8,128)(2,1)}, u32[]{:S(2)}) copy-start(bf16[256,128]{1,0:T(8,128)(2,1)} %get-tuple-element.17) | copy-start | bytes 196612
  50.7 4.5 %collective-permute-start = (bf16[256,128]{1,0:T(8,128)(2,1)S(1)}, bf16[256,128]{1,0:T(8,128)(2,1)S(1)}, u32[]{:S(2)}, u32[]{:S(2)}) collective-permute-start(bf16[256,128]{1,0:T(8,128)(2,1)S(1)} %copy-done.8), channel_id=1, source_target_pairs={{0,4},{4,0},{8,12},{12,8},{16,20},{20,16},{24,28},{28,24},{1,5},{5... | collective-permute-start | bytes 196616 | tf_op jit(solution)/shard_map/ppermute | solution.py:265
  55.2 2.4 %copy-start.6 = (bf16[256,128]{1,0:T(8,128)(2,1)}, bf16[256,128]{1,0:T(8,128)(2,1)S(1)}, u32[]{:S(2)}) copy-start(bf16[256,128]{1,0:T(8,128)(2,1)S(1)} %collective-permute-done.near_ref) | copy-start | bytes 196612
  57.6 0.7 copy-start.1
  57.6 0.8 %copy-start.4 = (bf16[512,384]{1,0:T(8,128)(2,1)}, bf16[512,384]{1,0:T(8,128)(2,1)S(1)}, u32[]{:S(2)}) copy-start(bf16[512,384]{1,0:T(8,128)(2,1)S(1)} %collective-permute-done.3.refs_2_) | copy-start | bytes 1179652
  57.6 0.9 %copy-start.5 = (bf16[512,384]{1,0:T(8,128)(2,1)}, bf16[512,384]{1,0:T(8,128)(2,1)S(1)}, u32[]{:S(2)}) copy-start(bf16[512,384]{1,0:T(8,128)(2,1)S(1)} %collective-permute-done.4.refs_3_) | copy-start | bytes 1179652
